TPU v7x, 32 devices: a whole 2x2x4 slice. The times are simulated.
32 devices in a mesh: sp: 8 (over z, y), tp: 4 (over x, core).
Axes of the slice: x: 2, y: 2, z: 4, core: 2. Of those that a mesh axis runs over, the one named last changes fastest.
Arguments:
- hidden: bfloat16 [2048, 4096], P('sp'), as said below
- key_weight: bfloat16 [4096, 1024], P(None, 'tp'), as said below
- queries: bfloat16 [2048, 4096], P('sp', 'tp'), as said below
- values: bfloat16 [2048, 1024], P('sp', 'tp'), as said below
- map_out: bfloat16 [2048, 8192], P('sp', 'tp'), as said below
- log_sums: float32 [32, 2048], P('tp', 'sp'), as said below
- out_grad: bfloat16 [2048, 4096], P('sp', 'tp'), may hold values from -6 to 6
- mixing: float32 [16], P('tp'), may hold values from 0.3 to 0.8
- out_gain: float32 [256], replicated, may hold values from 0.1 to 1.9
Outputs:
- grad_query: bfloat16 [2048, 4096], P('sp', 'tp')
- grad_key: bfloat16 [2048, 1024], P('sp', 'tp')
- grad_value: bfloat16 [2048, 1024], P('sp', 'tp')
- grad_weight: float32 [4096, 1024], P('sp', 'tp')
Inputs may be any that keep to these rules, and one draw needn't show every extreme that they name: `hidden`: inputs of order one. `key_weight`: entries of order 1 / sqrt(4096) times a constant. `queries`: entries of order one. `values`: entries of order one. `map_out`: for head h and map m: the row's weights exp(scores - log_sums) over keys j <= i times the values of key head g(h), rounded to bfloat16.
All inputs are finite; a program needn't handle non-finite values.
Results may differ from a plain program's by a relative error of at most 0.02.
Values may be sent and summed in bfloat16 or wider, within the bound.
A program may use at most 256 MiB of HBM per device.

v0:
```python
import functools
import math

import jax
import jax.numpy as jnp
from jax import lax
from jax.experimental import pallas as pl
from jax.experimental.pallas import tpu as pltpu
from jax.sharding import PartitionSpec as P

HEAD_DIM = 128
V_DIM = 256
OUT_SCALE = 0.8
NORM_EPS = 1e-06
LOG2E = math.log2(math.e)
VMEM = pltpu.VMEM


def dot_nn(a, b):
    return lax.dot_general(a, b, (((1,), (0,)), ((), ())), preferred_element_type=jnp.float32)


def dot_nt(a, b):
    return lax.dot_general(a, b, (((1,), (1,)), ((), ())), preferred_element_type=jnp.float32)


def dot_tn(a, b):
    return lax.dot_general(a, b, (((0,), (0,)), ((), ())), preferred_element_type=jnp.float32)


def head_terms(heads, og_ref, mo_ref, mix_ref, gain_ref, d_ref, term_ref):
    gain = gain_ref[...] * OUT_SCALE
    cols = []
    for h in range(heads):
        v_cols = pl.ds(h * V_DIM, V_DIM)
        map_a = mo_ref[:, pl.ds(2 * h * V_DIM, V_DIM)].astype(jnp.float32)
        map_b = mo_ref[:, pl.ds((2 * h + 1) * V_DIM, V_DIM)].astype(jnp.float32)
        pre = map_a - mix_ref[h] * map_b
        inv = lax.rsqrt(jnp.mean(pre * pre, axis=-1, keepdims=True) + NORM_EPS)
        up = og_ref[:, v_cols].astype(jnp.float32) * gain
        d_out = inv * (up - pre * (inv * inv * jnp.mean(up * pre, axis=-1, keepdims=True)))
        d_ref[:, v_cols] = d_out.astype(jnp.bfloat16)
        cols.append(jnp.sum(d_out * map_a, axis=-1, keepdims=True))
        cols.append(jnp.sum(d_out * map_b, axis=-1, keepdims=True))
    rows = cols[0].shape[0]
    lane = lax.broadcasted_iota(jnp.int32, (rows, 128), 1)
    packed = jnp.zeros((rows, 128), jnp.float32)
    for at, col in enumerate(cols):
        packed = jnp.where(lane == at, col, packed)
    term_ref[...] = packed.T[: 2 * heads]


def block_grads(heads, groups, k_ref, v_ref, q_ref, d_ref, log_ref, term_ref, mix_ref, gq_ref, masked):
    per_group = heads // groups
    scale = HEAD_DIM ** (-0.5)
    outs_k, outs_v = [], []
    for g in range(groups):
        keys = [k_ref[:, (2 * g + m) * HEAD_DIM : (2 * g + m + 1) * HEAD_DIM] for m in range(2)]
        keys_t = [k.T for k in keys]
        vals = v_ref[:, g * V_DIM : (g + 1) * V_DIM]
        grad_k = [None, None]
        grad_v = None
        for h in range(g * per_group, (g + 1) * per_group):
            mix = mix_ref[h]
            d_h = d_ref[:, h * V_DIM : (h + 1) * V_DIM]
            d_attn = dot_nt(vals, d_h)
            qs, probs = [], []
            for m in range(2):
                at = 2 * h + m
                q = q_ref[:, at * HEAD_DIM : (at + 1) * HEAD_DIM]
                s = dot_nt(keys[m], q)
                p = jnp.exp2(s * (scale * LOG2E) - log_ref[at : at + 1, :] * LOG2E)
                if masked:
                    k_at = lax.broadcasted_iota(jnp.int32, p.shape, 0)
                    q_at = lax.broadcasted_iota(jnp.int32, p.shape, 1)
                    p = jnp.where(k_at <= q_at, p, 0.0)
                qs.append(q)
                probs.append(p)
            mixed = mix * probs[1]
            w = (probs[0] - mixed).astype(jnp.bfloat16)
            ds = [
                (probs[0] * (d_attn - term_ref[2 * h : 2 * h + 1, :])).astype(jnp.bfloat16),
                (mixed * (term_ref[2 * h + 1 : 2 * h + 2, :] - d_attn)).astype(jnp.bfloat16),
            ]
            for m in range(2):
                at = 2 * h + m
                gq_ref[at * HEAD_DIM : (at + 1) * HEAD_DIM, :] += dot_nn(keys_t[m], ds[m])
                gk = dot_nn(ds[m], qs[m])
                grad_k[m] = gk if grad_k[m] is None else grad_k[m] + gk
            gv = dot_nn(w, d_h)
            grad_v = gv if grad_v is None else grad_v + gv
        outs_k += [gk * scale for gk in grad_k]
        outs_v.append(grad_v)
    return outs_k, outs_v


def attend_kernel(
    n, tp_count, heads, groups,
    hidden_ref, weight_ref, values_ref, q_ref, mo_ref, og_ref, log_ref, gain_ref, mix_ref,
    gq_out, gk_out, gv_out, gw_out,
    d_ref, term_ref, gq_ref, kv_ref, acc_ref, side_out, side_in, down_out, up_in, hid_ref, gk_ref,
    kv_recv, kv_up_sem, kv_side_sem, side_send, side_recv, down_send, up_recv,
    hid_send, hid_pass, hid_recv, gk_recv, gk_up_sem, gk_down_sem, gk_side_sem,
):
    me = lax.axis_index("sp")
    outer = n // 2
    o, y = me // 2, me % 2
    has_up = o < outer - 1
    up, down, side = me + 2, me - 2, me + 1 - 2 * y

    def kv_copy(b, part, sems, target, src=None):
        return pltpu.make_async_remote_copy(
            src_ref=kv_ref.at[b, part] if src is None else src,
            dst_ref=kv_ref.at[b, part],
            send_sem=sems.at[b // 2, part],
            recv_sem=kv_recv.at[b, part],
            device_id={"sp": target},
        )

    def side_copy(ob, part):
        return pltpu.make_async_remote_copy(
            src_ref=side_out.at[ob, part],
            dst_ref=side_in.at[ob, part],
            send_sem=side_send.at[ob, part],
            recv_sem=side_recv.at[ob, part],
            device_id={"sp": side},
        )

    def down_copy(ob, part):
        return pltpu.make_async_remote_copy(
            src_ref=down_out.at[ob, part],
            dst_ref=up_in.at[ob, part],
            send_sem=down_send.at[ob, part],
            recv_sem=up_recv.at[ob, part],
            device_id={"sp": down},
        )

    tp_at = lax.axis_index("tp")
    rows = q_ref.shape[0]
    part_rows = rows // tp_count
    wide = hidden_ref.shape[1] // n
    own_cols = pl.ds(pl.multiple_of(me * wide, wide), wide)
    own_rows = pl.ds(pl.multiple_of(tp_at * part_rows, part_rows), part_rows)

    def hid_slice(dest):
        return pltpu.make_async_remote_copy(
            src_ref=hidden_ref.at[own_rows, pl.ds(pl.multiple_of(dest * wide, wide), wide)],
            dst_ref=hid_ref.at[tp_at, me],
            send_sem=hid_send,
            recv_sem=hid_recv.at[tp_at],
            device_id={"sp": dest},
        )

    def hid_forward(source, target):
        return pltpu.make_async_remote_copy(
            src_ref=hid_ref.at[source],
            dst_ref=hid_ref.at[source],
            send_sem=hid_pass.at[target],
            recv_sem=hid_recv.at[source],
            device_id={"tp": target},
        )

    def hid_start():
        @pl.loop(1, n)
        def _(k):
            hid_slice((me + k) % n).start()

    def hid_wait(sem):
        pieces = hid_ref.at[tp_at, pl.ds(0, n - 1)]
        pltpu.make_async_copy(pieces, pieces, sem).wait()

    def hid_relay():
        hid_wait(hid_recv.at[tp_at])

        @pl.loop(1, tp_count)
        def _(k):
            hid_forward(tp_at, (tp_at + k) % tp_count).start()

    def gk_copy(b, sems, target):
        return pltpu.make_async_remote_copy(
            src_ref=gk_ref.at[b],
            dst_ref=gk_ref.at[b],
            send_sem=sems.at[b // 2],
            recv_sem=gk_recv.at[b],
            device_id={"sp": target},
        )

    def gk_each(b, act):
        ob = b // 2

        @pl.when((ob <= o) & has_up)
        def _():
            act(gk_copy(b, gk_up_sem, up))

        @pl.when((ob >= o) & (o > 0))
        def _():
            act(gk_copy(b, gk_down_sem, down))

        act(gk_copy(b, gk_side_sem, side))

    def add_weight(b):
        block = jnp.concatenate([hid_ref[k, b] for k in range(tp_count)], axis=0)
        gw_out[...] += dot_tn(block, gk_ref[b])

    barrier = pltpu.get_barrier_semaphore()

    @pl.loop(1, n)
    def _(k):
        pl.semaphore_signal(barrier, inc=1, device_id={"sp": (me + k) % n})

    @pl.loop(1, tp_count)
    def _(k):
        pl.semaphore_signal(barrier, inc=1, device_id={"tp": (tp_at + k) % tp_count})

    pl.semaphore_wait(barrier, n + tp_count - 2)

    def start_own(part, src=None):
        @pl.when(has_up)
        def _():
            kv_copy(me, part, kv_up_sem, up, src).start()

        @pl.when(y == 0)
        def _():
            kv_copy(me, part, kv_side_sem, side, src).start()

    start_own(1, values_ref)
    kv_ref[me, 0] = dot_nn(hidden_ref[...], weight_ref[...]).astype(jnp.bfloat16)
    kv_ref[me, 1] = values_ref[...]
    start_own(0)
    hid_ref[tp_at, me] = hidden_ref[own_rows, own_cols]

    @pl.when(~has_up)
    def _():
        hid_start()

    head_terms(heads, og_ref, mo_ref, mix_ref, gain_ref, d_ref, term_ref)
    gw_out[...] = jnp.zeros_like(gw_out)
    gq_ref[...] = jnp.zeros_like(gq_ref)

    def grads(b, masked):
        return block_grads(
            heads, groups, kv_ref.at[b, 0], kv_ref.at[b, 1], q_ref, d_ref, log_ref, term_ref, mix_ref, gq_ref, masked
        )

    def store(ref, ob, pieces):
        for part in range(2):
            at = 0
            for piece in pieces[part]:
                ref[ob, part, :, at : at + piece.shape[1]] = piece.astype(ref.dtype)
                at += piece.shape[1]

    lag = jnp.where(has_up, o + 2, 2)

    @pl.loop(0, o + lag + 1)
    def _(t):
        @pl.when(t == 0)
        def _():
            store(acc_ref, o, grads(me, True))

        @pl.when((t > 0) & (t <= o))
        def _():
            b = me - 2 * t
            for part in (1, 0):
                kv_copy(b, part, kv_up_sem, up).wait_recv()

                @pl.when(has_up)
                def _():
                    kv_copy(b, part, kv_up_sem, up).start()

                kv_copy(b, part, kv_side_sem, side).start()
            store(acc_ref, o - t, grads(b, False))

        @pl.when((t > 0) & (t <= o + 1) & ((t > 1) | (y == 1)))
        def _():
            ob = o - t + 1
            b = 2 * ob + 1 - y
            for part in (1, 0):
                kv_copy(b, part, kv_side_sem, side).wait_recv()
            store(side_out, ob, grads(b, False))
            for part in range(2):
                side_copy(ob, part).start()

        @pl.when((t == o + 1) & has_up)
        def _():
            hid_start()

        @pl.when((t == o + 2) & has_up)
        def _():
            hid_relay()

        @pl.when(t >= lag)
        def _():
            ob = o - t + lag
            for part in range(2):
                @pl.when((ob < o) | (y == 0))
                def _():
                    side_copy(ob, part).wait_recv()
                    acc_ref[ob, part] += side_in[ob, part].astype(jnp.float32)

                @pl.when(has_up)
                def _():
                    down_copy(ob, part).wait_recv()
                    acc_ref[ob, part] += up_in[ob, part].astype(jnp.float32)

                if part == 0:
                    @pl.when(ob == o)
                    def _():
                        gk_ref[me] = acc_ref[o, 0].astype(jnp.bfloat16)
                        gk_each(me, lambda copy: copy.start())

                @pl.when(ob < o)
                def _():
                    down_out[ob, part] = acc_ref[ob, part].astype(jnp.bfloat16)
                    down_copy(ob, part).start()

        @pl.when(t == o + 1)
        def _():
            for at in range(2 * heads):
                cols = slice(at * HEAD_DIM, (at + 1) * HEAD_DIM)
                gq_out[:, cols] = (gq_ref[cols, :] * HEAD_DIM ** (-0.5)).T.astype(gq_out.dtype)

    @pl.when(~has_up)
    def _():
        hid_relay()

    gk_out[...] = gk_ref[me]
    gv_out[...] = acc_ref[o, 1].astype(gv_out.dtype)

    @pl.loop(1, tp_count)
    def _(k):
        hid_forward((tp_at + k) % tp_count, tp_at).wait_recv()

    add_weight(me)

    @pl.loop(0, outer)
    def _(k):
        b = 2 * (outer - 1 - k) + y

        @pl.when(b != me)
        def _():
            gk_copy(b, gk_side_sem, side).wait_recv()
            gk_each(b, lambda copy: copy.start())
            add_weight(b)

    @pl.loop(0, outer)
    def _(k):
        b = 2 * (outer - 1 - k) + 1 - y
        gk_copy(b, gk_side_sem, side).wait_recv()
        add_weight(b)

    hid_wait(hid_send)

    @pl.loop(1, tp_count)
    def _(k):
        hid_forward(tp_at, (tp_at + k) % tp_count).wait_send()

    @pl.loop(0, outer)
    def _(ob):
        gk_each(2 * ob + y, lambda copy: copy.wait_send())

    @pl.loop(0, o + 1)
    def _(ob):
        for part in range(2):
            @pl.when(has_up)
            def _():
                kv_copy(2 * ob + y, part, kv_up_sem, up).wait_send()

            @pl.when((ob < o) | (y == 0))
            def _():
                kv_copy(2 * ob + y, part, kv_side_sem, side).wait_send()

            @pl.when((ob < o) | (y == 1))
            def _():
                side_copy(ob, part).wait_send()

            @pl.when(ob < o)
            def _():
                down_copy(ob, part).wait_send()


def write_kernel(*refs):
    for src, dst in zip(refs[:4], refs[4:]):
        dst[...] = src[...]


def on_device(n, tp_count, hidden, key_weight, queries, values, map_out, log_sums, out_grad, mixing, out_gain):
    rows = queries.shape[0]
    heads = mixing.shape[0]
    width = values.shape[1]
    groups = width // V_DIM
    outer = n // 2
    vm = pl.BlockSpec(memory_space=VMEM)
    hops = pltpu.SemaphoreType.DMA((outer, 2))
    results = pl.pallas_call(
        functools.partial(attend_kernel, n, tp_count, heads, groups),
        out_shape=(
            jax.ShapeDtypeStruct(queries.shape, jnp.bfloat16),
            jax.ShapeDtypeStruct((rows, width), jnp.bfloat16),
            jax.ShapeDtypeStruct((rows, width), jnp.bfloat16),
            jax.ShapeDtypeStruct((hidden.shape[1] // n, width), jnp.float32),
        ),
        in_specs=[vm] * 8 + [pl.BlockSpec(memory_space=pltpu.SMEM)],
        out_specs=(vm, vm, vm, vm),
        scratch_shapes=[
            VMEM((rows, heads * V_DIM), jnp.bfloat16),
            VMEM((2 * heads, rows), jnp.float32),
            VMEM((2 * heads * HEAD_DIM, rows), jnp.float32),
            VMEM((n, 2, rows, width), jnp.bfloat16),
            VMEM((outer, 2, rows, width), jnp.float32),
        ]
        + [VMEM((outer, 2, rows, width), jnp.bfloat16)] * 4
        + [
            VMEM((tp_count, n, rows // tp_count, hidden.shape[1] // n), jnp.bfloat16),
            VMEM((n, rows, width), jnp.bfloat16),
        ]
        + [pltpu.SemaphoreType.DMA((n, 2))]
        + [hops] * 6
        + [pltpu.SemaphoreType.DMA]
        + [pltpu.SemaphoreType.DMA((size,)) for size in (tp_count, tp_count, n, outer, outer, outer)],
        compiler_params=pltpu.CompilerParams(
            vmem_limit_bytes=60 * 2**20, collective_id=0, has_side_effects=True
        ),
        cost_estimate=pl.CostEstimate(flops=5 * 10**9, bytes_accessed=10**7, transcendentals=0),
    )(hidden, key_weight, values, queries, map_out, out_grad, log_sums, out_gain.reshape(1, V_DIM), mixing)
    return pl.pallas_call(
        write_kernel,
        out_shape=tuple(jax.ShapeDtypeStruct(r.shape, r.dtype) for r in results),
        in_specs=[vm] * 4,
        out_specs=(vm,) * 4,
        cost_estimate=pl.CostEstimate(flops=10**6, bytes_accessed=4 * 10**6, transcendentals=0),
    )(*results)


def solution(mesh):
    placed = (
        P("sp", None),
        P(None, "tp"),
        P("sp", "tp"),
        P("sp", "tp"),
        P("sp", "tp"),
        P("tp", "sp"),
        P("sp", "tp"),
        P("tp"),
        P(),
    )
    return jax.shard_map(
        functools.partial(on_device, mesh.shape["sp"], mesh.shape["tp"]),
        mesh=mesh,
        in_specs=placed,
        out_specs=(P("sp", "tp"), P("sp", "tp"), P("sp", "tp"), P("sp", "tp")),
        check_vma=False,
    )
```

profile of v0, /device:TPU:25, one launch (start us, length us, event | category | flops | bytes accessed | tf_op | source)
XLA Modules:
  0.0 92.1 jit_solution(8621474142234497390)
XLA Ops:
  0.6 89.1 %shard_map.120 = (bf16[256,1024]{1,0:T(8,128)(2,1)}, bf16[256,256]{1,0:T(8,128)(2,1)}, bf16[256,256]{1,0:T(8,128)(2,1)}, f32[512,256]{1,0:T(8,128)}) custom-call(bf16[256,4096]{1,0:T(8,128)(2,1)} %hidden_ref.1, bf16[4096,256]{1,0:T(8,128)(2,1)} %weight_ref.1, bf16[256,256]{1,0:T(8,128)(2,1)} %values_ref.1, bf16[256,1024]{1,0:T(8,128)(2,1)} %q_ref.1, ...), custom_call_target="tpu_custom_call" | custom-call | flops 5000000000 | bytes 10000000 | tf_op jit(solution)/shard_map/pallas_call | solution.py:394
  89.8 2.4 %shard_map.121 = (bf16[256,1024]{1,0:T(8,128)(2,1)}, bf16[256,256]{1,0:T(8,128)(2,1)}, bf16[256,256]{1,0:T(8,128)(2,1)}, f32[512,256]{1,0:T(8,128)}) custom-call(bf16[256,1024]{1,0:T(8,128)(2,1)} %get-tuple-element.8.refs_0_, bf16[256,256]{1,0:T(8,128)(2,1)} %get-tuple-element.9.refs_1_, bf16[256,256]{1,0:T(8,128)(2,1)} %get-tuple-element.10.refs_2_, ...), custom_call_target="tpu_custom_call" | custom-call | flops 1000000 | bytes 4000000 | tf_op jit(solution)/shard_map/pallas_call | solution.py:425
where the time goes:
time: 93.3 us; the launch traced here: 92.1 us
  Pallas kernels  91.5 us (98%)
    pallas_call x1, Pallas kernels, on_device(): pl.pallas_call(functools.partial(attend_kernel, n, tp_count, heads, group...  89.1 us
    pallas_call x1, Pallas kernels, on_device(): pl.pallas_call(write_kernel, out_shape=tuple((jax.ShapeDtypeStruct(r.shap...  2.38 us

commit v1 on v0

v1 whole, which is shorter than its diff:
```python
import functools
import math

import jax
import jax.numpy as jnp
from jax import lax
from jax.experimental import pallas as pl
from jax.experimental.pallas import tpu as pltpu
from jax.sharding import PartitionSpec as P

HEAD_DIM = 128
V_DIM = 256
OUT_SCALE = 0.8
NORM_EPS = 1e-06
LOG2E = math.log2(math.e)
SCALE = HEAD_DIM ** (-0.5)
VMEM = pltpu.VMEM
DMA = pltpu.SemaphoreType.DMA


def dot_nn(a, b):
    return lax.dot_general(a, b, (((1,), (0,)), ((), ())), preferred_element_type=jnp.float32)


def dot_nt(a, b):
    return lax.dot_general(a, b, (((1,), (1,)), ((), ())), preferred_element_type=jnp.float32)


def dot_tn(a, b):
    return lax.dot_general(a, b, (((0,), (0,)), ((), ())), preferred_element_type=jnp.float32)


def head_terms(pair, half, slot, og_ref, mo_ref, log_ref, mix_ref, gain_ref, d_ref, m_ref):
    gain = gain_ref[...] * OUT_SCALE
    rows = og_ref.shape[0]
    cols, lifts = [], []
    for i in range(half):
        h = pair * half + i
        at = pl.multiple_of(2 * h * V_DIM, V_DIM)
        map_a = mo_ref[:, pl.ds(at, V_DIM)].astype(jnp.float32)
        map_b = mo_ref[:, pl.ds(at + V_DIM, V_DIM)].astype(jnp.float32)
        pre = map_a - mix_ref[h] * map_b
        inv = lax.rsqrt(jnp.mean(pre * pre, axis=-1, keepdims=True) + NORM_EPS)
        up = og_ref[:, pl.ds(pl.multiple_of(h * V_DIM, V_DIM), V_DIM)].astype(jnp.float32) * gain
        d_out = inv * (up - pre * (inv * inv * jnp.mean(up * pre, axis=-1, keepdims=True)))
        d_ref[slot, :, i * V_DIM : (i + 1) * V_DIM] = d_out.astype(jnp.bfloat16)
        cols.append(jnp.sum(d_out * map_a, axis=-1, keepdims=True))
        cols.append(jnp.sum(d_out * map_b, axis=-1, keepdims=True))
        lifts.append(jnp.zeros((1, rows), jnp.float32))
        lifts.append(jnp.log(jnp.full((1, rows), mix_ref[h], jnp.float32)))
    lane = lax.broadcasted_iota(jnp.int32, (rows, 128), 1)
    packed = jnp.zeros((rows, 128), jnp.float32)
    for at, col in enumerate(cols):
        packed = jnp.where(lane == at, col, packed)
    logs = log_ref[...]
    logs = jnp.where(pair == 0, logs[: 2 * half], logs[2 * half :])
    m_ref[slot, : 2 * half] = (logs - jnp.concatenate(lifts, axis=0)) * LOG2E
    m_ref[slot, 2 * half :] = packed.T[: 2 * half]


def block_grads(half, slots, k_ref, v_ref, q_ref, d_ref, m_ref, gq_ref, masked):
    keys = [k_ref[:, m * HEAD_DIM : (m + 1) * HEAD_DIM] for m in range(2)]
    keys_t = [k.T for k in keys]
    vals = v_ref[...]
    grad_k = [None, None]
    grad_v = None
    for slot in slots:
        for i in range(half):
            d_h = d_ref[slot, :, i * V_DIM : (i + 1) * V_DIM]
            d_attn = dot_nt(vals, d_h)
            qs, probs, terms = [], [], []
            for m in range(2):
                at = 2 * i + m
                q = q_ref[slot, :, at * HEAD_DIM : (at + 1) * HEAD_DIM]
                p = jnp.exp2(dot_nt(keys[m], q) * (SCALE * LOG2E) - m_ref[slot, at : at + 1, :])
                if masked:
                    k_at = lax.broadcasted_iota(jnp.int32, p.shape, 0)
                    q_at = lax.broadcasted_iota(jnp.int32, p.shape, 1)
                    p = jnp.where(k_at <= q_at, p, 0.0)
                qs.append(q)
                probs.append(p)
                terms.append(m_ref[slot, 2 * half + at : 2 * half + at + 1, :])
            w = (probs[0] - probs[1]).astype(jnp.bfloat16)
            ds = [
                (probs[0] * (d_attn - terms[0])).astype(jnp.bfloat16),
                (probs[1] * (terms[1] - d_attn)).astype(jnp.bfloat16),
            ]
            for m in range(2):
                at = 2 * i + m
                gq_ref[slot, at * HEAD_DIM : (at + 1) * HEAD_DIM, :] += dot_nn(keys_t[m], ds[m])
                gk = dot_nn(ds[m], qs[m])
                grad_k[m] = gk if grad_k[m] is None else grad_k[m] + gk
            gv = dot_nn(w, d_h)
            grad_v = gv if grad_v is None else grad_v + gv
    return grad_k, grad_v


def attend_kernel(
    n, tp_count, heads,
    hidden_ref, weight_ref, values_ref, q_in_ref, mo_in_ref, og_in_ref, log_ref, gain_ref, mix_ref,
    gq_out, gk_out, gv_out, gw_out,
    hid_vm, w_vm, mo_vm, og_vm, qb, db, mb, kv, acc, keep, p_out, p_in, up_in, dn_out,
    gkb, gv_fin, gv_in, gq_t, gq_fin, gq_in, hid,
    load_sem, q_send, q_recv, d_send, d_recv, m_send, m_recv,
    kv_recv, kv_own, kv_up, kv_pair, p_send, p_recv, dn_send, up_recv,
    gk_recv, gk_up, gk_dn, gk_pair, gk_cross, gv_send, gv_recv, gq_send, gq_recv,
    hid_send, hid_recv, hid_pass, hid_pair,
):
    me = lax.axis_index("sp")
    tp = lax.axis_index("tp")
    outer = n // 2
    half = heads // 2
    o, y = me // 2, me % 2
    x, c = tp // 2, tp % 2
    mate, pair = me + 1 - 2 * y, tp + 1 - 2 * c
    has_up = o < outer - 1
    home = y == c
    rows = og_in_ref.shape[0]
    hrows = rows // 2
    pair_q, pair_v = half * 2 * HEAD_DIM, half * V_DIM

    def remote(src, dst, send, recv, sp=me, to=tp):
        return pltpu.make_async_remote_copy(
            src_ref=src, dst_ref=dst, send_sem=send, recv_sem=recv, device_id={"sp": sp, "tp": to}
        )

    def landed(ref, sem):
        pltpu.make_async_copy(ref, ref, sem).wait()

    own_kv = jnp.where(home, me, n)

    def slot_of(p):
        return jnp.where(home & (p == c), y, 2 + p)

    def load(k):
        if k < 2:
            return pltpu.make_async_copy(
                q_in_ref.at[:, pl.ds(k * pair_q, pair_q)], qb.at[slot_of(k)], load_sem.at[k]
            )
        src, dst = {
            2: (values_ref, kv.at[own_kv, 1]),
            3: (hidden_ref, hid_vm),
            4: (weight_ref, w_vm),
            5: (mo_in_ref, mo_vm),
            6: (og_in_ref, og_vm),
        }[k]
        return pltpu.make_async_copy(src, dst, load_sem.at[k])

    for k in (2, 3, 4, 0, 1, 5, 6):
        load(k).start()

    barrier = pltpu.get_barrier_semaphore()

    @pl.loop(1, n)
    def _(k):
        pl.semaphore_signal(barrier, inc=1, device_id={"sp": (me + k) % n})

    @pl.loop(1, tp_count)
    def _(k):
        pl.semaphore_signal(barrier, inc=1, device_id={"tp": (tp + k) % tp_count})

    pl.semaphore_signal(barrier, inc=1, device_id={"sp": mate, "tp": pair})
    pl.semaphore_wait(barrier, n + tp_count - 1)

    def spread(buf, p, send, recv):
        return remote(buf.at[2 + p], buf.at[y], send.at[p], recv.at[y], 2 * o + c, 2 * x + p)

    def not_self(p):
        return ~(home & (p == c))

    def arrive(buf, slot, recv):
        landed(buf.at[slot], recv.at[slot])

    def rows_arrive(slot):
        arrive(qb, slot, q_recv)
        arrive(db, slot, d_recv)
        arrive(mb, slot, m_recv)

    def own_copy(p):
        return remote(
            kv.at[own_kv, p], kv.at[me, p], kv_own.at[p], kv_recv.at[me, p],
            2 * o + c, 2 * x + jnp.where(home, 1 - c, p),
        )

    def up_copy(b):
        return remote(kv.at[b, c], kv.at[b, c], kv_up.at[b], kv_recv.at[b, c], me + 2)

    def pair_copy(b):
        return remote(kv.at[b, c], kv.at[b, c], kv_pair.at[b], kv_recv.at[b, c], me, pair)

    def kv_wait(b, p):
        landed(kv.at[b, p], kv_recv.at[b, p])

    def pass_up(b):
        @pl.when(has_up)
        def _():
            up_copy(b).start()

    def take(b):
        kv_wait(b, c)
        pass_up(b)
        pair_copy(b).start()

    part_rows = rows // tp_count
    wide = hid_vm.shape[1] // n
    own_rows = pl.ds(pl.multiple_of(tp * part_rows, part_rows), part_rows)

    def columns(dest):
        return pl.ds(pl.multiple_of(dest * wide, wide), wide)

    def hid_slice(dest):
        return remote(hid_vm.at[own_rows, columns(dest)], hid.at[tp, me], hid_send, hid_recv.at[tp], dest)

    def hid_early():
        @pl.loop(0, o)
        def _(l):
            hid_slice(2 * l + y).start()

    def hid_late():
        @pl.loop(1, n)
        def _(k):
            dest = (me + k) % n

            @pl.when((dest // 2 >= o) | (dest % 2 != y))
            def _():
                hid_slice(dest).start()

    def hid_wait(sem):
        pieces = hid.at[tp, pl.ds(0, n - 1)]
        pltpu.make_async_copy(pieces, pieces, sem).wait()

    def hid_over(k):
        return remote(hid.at[tp], hid.at[tp], hid_pass.at[k], hid_recv.at[tp], me, (tp + 2 * k) % tp_count)

    def hid_to_pair(k):
        source = (tp + 2 * k) % tp_count
        return remote(hid.at[source], hid.at[source], hid_pair.at[k], hid_recv.at[source], me, pair)

    load(2).wait()
    own_copy(1).start()

    @pl.when(home & (c == 1) & has_up)
    def _():
        up_copy(me).start()

    for p in range(2):
        load(p).wait()

    def send_q(p):
        @pl.when(not_self(p))
        def _():
            spread(qb, p, q_send, q_recv).start()

    send_q(0)
    load(3).wait()
    load(4).wait()
    kv[own_kv, 0] = dot_nn(hid_vm[...], w_vm[...]).astype(jnp.bfloat16)
    own_copy(0).start()

    @pl.when(home & (c == 0) & has_up)
    def _():
        up_copy(me).start()

    send_q(1)
    load(5).wait()
    load(6).wait()

    @pl.loop(0, 2)
    def _(k):
        p = jnp.where(k == 0, 1 - c, c)
        head_terms(p, half, slot_of(p), og_vm, mo_vm, log_ref, mix_ref, gain_ref, db, mb)

        @pl.when(not_self(p))
        def _():
            spread(db, p, d_send, d_recv).start()
            spread(mb, p, m_send, m_recv).start()

    hid[tp, me] = hid_vm[own_rows, columns(me)]
    hid_early()
    gw_out[...] = jnp.zeros_like(gw_out)
    gq_t[...] = jnp.zeros_like(gq_t)

    def grads(b, slots, masked=False):
        grad_k, grad_v = block_grads(half, slots, kv.at[b, 0], kv.at[b, 1], qb, db, mb, gq_t, masked)
        return [(0, 0, grad_k[0]), (0, HEAD_DIM, grad_k[1]), (1, 0, grad_v)]

    def hold(at, pieces, add):
        for part, col, piece in pieces:
            cols = pl.ds(col, piece.shape[1])
            if add:
                acc[at, part, :, cols] += piece
            else:
                acc[at, part, :, cols] = piece

    def partial(b):
        return remote(p_out.at[b], p_in.at[b], p_send.at[b], p_recv.at[b], me, pair)

    def emit(b, pieces):
        for part, col, piece in pieces:
            cols = pl.ds(col, piece.shape[1])
            lo, hi = piece[:hrows], piece[hrows:]
            keep[b, part, :, cols] = jnp.where(c == 0, lo, hi)
            p_out[b, part, :, cols] = jnp.where(c == 0, hi, lo).astype(jnp.bfloat16)
        partial(b).start()

    def held(at):
        return [(part, 0, acc[at, part]) for part in range(2)]

    carried = jnp.where(home, c, 2)

    def down(b, part):
        return remote(dn_out.at[b, part], up_in.at[b, part], dn_send.at[b, part], up_recv.at[b, part], me - 2)

    def gk_hop(b, sems, target):
        return remote(gkb.at[b, carried], gkb.at[b, carried], sems.at[b], gk_recv.at[b, carried], target)

    def gk_give(b, sems, target, to):
        return remote(gkb.at[b, carried], gkb.at[b, c], sems.at[b], gk_recv.at[b, c], target, to)

    def gk_deliver(b, act):
        act(gk_give(b, gk_cross, mate, 2 * x + y))

        @pl.when(~home)
        def _():
            act(gk_give(b, gk_pair, me, pair))

    def gk_up_hop(b, act):
        @pl.when(has_up)
        def _():
            act(gk_hop(b, gk_up, me + 2))

    def gk_dn_hop(b, act):
        @pl.when(o > 0)
        def _():
            act(gk_hop(b, gk_dn, me - 2))

    def start(copy):
        copy.start()

    def gv_give(s):
        return remote(gv_fin.at[s], gv_in.at[c], gv_send.at[s], gv_recv.at[c], 2 * o + s, 2 * x + y)

    def each_of(level, act):
        @pl.loop(0, 2)
        def _(j):
            act(2 * level + jnp.where(j == 0, y, 1 - y))

    def reduce(b):
        landed(p_in.at[b], p_recv.at[b])
        for part in range(2):
            @pl.when(has_up)
            def _():
                landed(up_in.at[b, part], up_recv.at[b, part])
                keep[b, part] += up_in[b, part].astype(jnp.float32)

            total = keep[b, part] + p_in[b, part].astype(jnp.float32)

            @pl.when(b // 2 < o)
            def _():
                dn_out[b, part] = total.astype(jnp.bfloat16)
                down(b, part).start()

            @pl.when(b // 2 == o)
            def _():
                if part == 0:
                    gkb[b, carried] = (total * SCALE).astype(jnp.bfloat16)
                    gk_up_hop(b, start)
                    gk_dn_hop(b, start)
                    gk_deliver(b, start)
                else:
                    s = b % 2

                    @pl.when(home & (s == y))
                    def _():
                        gv_in[c] = total.astype(jnp.bfloat16)

                    @pl.when(~(home & (s == y)))
                    def _():
                        gv_fin[s] = total.astype(jnp.bfloat16)
                        gv_give(s).start()

    @pl.when(~home)
    def _():
        kv_wait(me, c)
        pass_up(me)
        rows_arrive(y)
        kv_wait(me, 1 - c)

    hold(y, grads(me, [y], True), False)
    take(mate)

    @pl.when(o > 0)
    def _():
        @pl.loop(0, 2)
        def _(j):
            b = 2 * (o - 1) + jnp.where(j == 0, y, 1 - y)
            take(b)
            kv_wait(b, 1 - c)
            hold(2 + b % 2, grads(b, [y]), False)

    kv_wait(mate, 1 - c)
    rows_arrive(1 - y)
    hold(1 - y, grads(mate, [1 - y], True), False)
    hold(0, grads(2 * o, [1]), True)
    emit(2 * o, held(0))
    emit(2 * o + 1, held(1))

    @pl.when(o > 0)
    def _():
        @pl.loop(0, 2)
        def _(j):
            b = 2 * (o - 1) + jnp.where(j == 0, y, 1 - y)
            hold(2 + b % 2, grads(b, [1 - y]), True)
            emit(b, held(2 + b % 2))

            @pl.when((j == 0) & ~has_up)
            def _():
                each_of(o, reduce)

    @pl.loop(2, o + 1)
    def _(t):
        @pl.loop(0, 2)
        def _(j):
            b = 2 * (o - t) + jnp.where(j == 0, y, 1 - y)
            take(b)
            kv_wait(b, 1 - c)
            emit(b, grads(b, [0, 1]))

            @pl.when((j == 0) & ~has_up)
            def _():
                each_of(o - t + 1, reduce)

    @pl.when(~has_up)
    def _():
        each_of(0, reduce)

    hid_late()

    def gq_give(s):
        return remote(gq_fin.at[s], gq_in.at[c], gq_send.at[s], gq_recv.at[c], 2 * o + s, 2 * x + y)

    @pl.loop(0, 2)
    def _(k):
        s = jnp.where(k == 0, 1 - y, y)
        local = home & (s == y)
        for at in range(2 * half):
            cols = slice(at * HEAD_DIM, (at + 1) * HEAD_DIM)
            piece = (gq_t[s, cols, :] * SCALE).T.astype(jnp.bfloat16)

            @pl.when(local)
            def _():
                gq_in[c, :, cols] = piece

            @pl.when(~local)
            def _():
                gq_fin[s, :, cols] = piece

        @pl.when(~local)
        def _():
            gq_give(s).start()

    @pl.when(has_up)
    def _():
        each_of(o, reduce)

    @pl.loop(o + 1, outer)
    def _(l):
        def step(b):
            landed(gkb.at[b, carried], gk_recv.at[b, carried])
            gk_dn_hop(b, start)
            gk_deliver(b, start)

        each_of(l, step)

    hid_wait(hid_recv.at[tp])

    @pl.loop(1, tp_count // 2)
    def _(k):
        hid_over(k).start()

    hid_to_pair(0).start()

    @pl.when(has_up)
    def _():
        @pl.loop(0, o)
        def _(k):
            each_of(o - 1 - k, reduce)

    @pl.loop(1, tp_count // 2)
    def _(k):
        source = (tp + 2 * k) % tp_count
        landed(hid.at[source], hid_recv.at[source])
        hid_to_pair(k).start()

    @pl.loop(0, tp_count // 2)
    def _(k):
        source = (pair + 2 * k) % tp_count
        landed(hid.at[source], hid_recv.at[source])

    def gk_ready(b):
        for h in range(2):
            @pl.when(~(home & (c == h)))
            def _():
                landed(gkb.at[b, h], gk_recv.at[b, h])

    def add_weight(b):
        gk_ready(b)
        block = jnp.concatenate([hid[k, b] for k in range(tp_count)], axis=0)
        gw_out[...] += dot_tn(block, jnp.concatenate([gkb[b, 0], gkb[b, 1]], axis=0))

    @pl.loop(0, outer)
    def _(k):
        l = jnp.where(k < outer - o, o + k, outer - 1 - k)

        @pl.when(l < o)
        def _():
            def step(b):
                landed(gkb.at[b, carried], gk_recv.at[b, carried])
                gk_up_hop(b, start)
                gk_deliver(b, start)

            each_of(l, step)

        each_of(l, add_weight)

    gk_out[:hrows] = gkb[me, 0]
    gk_out[hrows:] = gkb[me, 1]
    for h in range(2):
        @pl.when(~(home & (c == h)))
        def _():
            landed(gv_in.at[h], gv_recv.at[h])
            landed(gq_in.at[h], gq_recv.at[h])

        gv_out[h * hrows : (h + 1) * hrows] = gv_in[h]
        gq_out[:, h * pair_q : (h + 1) * pair_q] = gq_in[h]

    for p in range(2):
        own_copy(p).wait_send()

        @pl.when(not_self(p))
        def _():
            spread(qb, p, q_send, q_recv).wait_send()
            spread(db, p, d_send, d_recv).wait_send()
            spread(mb, p, m_send, m_recv).wait_send()

        @pl.when(~(home & (y == p)))
        def _():
            gv_give(p).wait_send()
            gq_give(p).wait_send()

    @pl.loop(0, 2 * o + 2)
    def _(b):
        @pl.when(has_up)
        def _():
            up_copy(b).wait_send()

        @pl.when(b != me)
        def _():
            pair_copy(b).wait_send()

        partial(b).wait_send()

        @pl.when(b // 2 < o)
        def _():
            for part in range(2):
                down(b, part).wait_send()

    @pl.loop(0, n)
    def _(b):
        @pl.when(b // 2 <= o)
        def _():
            gk_up_hop(b, lambda copy: copy.wait_send())

        @pl.when(b // 2 >= o)
        def _():
            gk_dn_hop(b, lambda copy: copy.wait_send())

        gk_deliver(b, lambda copy: copy.wait_send())

    hid_wait(hid_send)

    @pl.loop(1, tp_count // 2)
    def _(k):
        hid_over(k).wait_send()

    @pl.loop(0, tp_count // 2)
    def _(k):
        hid_to_pair(k).wait_send()


def write_kernel(*refs):
    for src, dst in zip(refs[:4], refs[4:]):
        dst[...] = src[...]


def on_device(n, tp_count, hidden, key_weight, queries, values, map_out, log_sums, out_grad, mixing, out_gain):
    rows = queries.shape[0]
    heads = mixing.shape[0]
    width = values.shape[1]
    half = heads // 2
    hrows = rows // 2
    assert width == V_DIM and n % 2 == 0 and tp_count % 2 == 0 and n >= 4
    bf16, f32 = jnp.bfloat16, jnp.float32
    vm = pl.BlockSpec(memory_space=VMEM)
    hbm = pl.BlockSpec(memory_space=pl.ANY)
    buffers = [
        VMEM(hidden.shape, bf16),
        VMEM(key_weight.shape, bf16),
        VMEM(map_out.shape, bf16),
        VMEM(out_grad.shape, bf16),
        VMEM((4, rows, half * 2 * HEAD_DIM), bf16),
        VMEM((4, rows, half * V_DIM), bf16),
        VMEM((4, 4 * half, rows), f32),
        VMEM((n + 1, 2, rows, width), bf16),
        VMEM((4, 2, rows, width), f32),
        VMEM((n, 2, hrows, width), f32),
        VMEM((n, 2, hrows, width), bf16),
        VMEM((n, 2, hrows, width), bf16),
        VMEM((n, 2, hrows, width), bf16),
        VMEM((n, 2, hrows, width), bf16),
        VMEM((n, 3, hrows, width), bf16),
        VMEM((2, hrows, width), bf16),
        VMEM((2, hrows, width), bf16),
        VMEM((2, half * 2 * HEAD_DIM, rows), f32),
        VMEM((2, rows, half * 2 * HEAD_DIM), bf16),
        VMEM((2, rows, half * 2 * HEAD_DIM), bf16),
        VMEM((tp_count, n, rows // tp_count, hidden.shape[1] // n), bf16),
    ]
    sems = [
        DMA((7,)),
        *[DMA((2,))] * 6,
        DMA((n, 2)),
        DMA((2,)),
        DMA((n,)),
        DMA((n,)),
        DMA((n,)),
        DMA((n,)),
        DMA((n, 2)),
        DMA((n, 2)),
        DMA((n, 3)),
        *[DMA((n,))] * 4,
        *[DMA((2,))] * 4,
        DMA,
        *[DMA((tp_count,))] * 3,
    ]
    results = pl.pallas_call(
        functools.partial(attend_kernel, n, tp_count, heads),
        out_shape=(
            jax.ShapeDtypeStruct(queries.shape, bf16),
            jax.ShapeDtypeStruct((rows, width), bf16),
            jax.ShapeDtypeStruct((rows, width), bf16),
            jax.ShapeDtypeStruct((hidden.shape[1] // n, width), f32),
        ),
        in_specs=[hbm] * 6 + [vm] * 2 + [pl.BlockSpec(memory_space=pltpu.SMEM)],
        out_specs=(vm, vm, vm, vm),
        scratch_shapes=buffers + sems,
        compiler_params=pltpu.CompilerParams(
            vmem_limit_bytes=60 * 2**20, collective_id=0, has_side_effects=True
        ),
        cost_estimate=pl.CostEstimate(flops=5 * 10**9, bytes_accessed=10**7, transcendentals=0),
    )(hidden, key_weight, values, queries, map_out, out_grad, log_sums, out_gain.reshape(1, V_DIM), mixing)
    return pl.pallas_call(
        write_kernel,
        out_shape=tuple(jax.ShapeDtypeStruct(r.shape, r.dtype) for r in results),
        in_specs=[vm] * 4,
        out_specs=(vm,) * 4,
        cost_estimate=pl.CostEstimate(flops=10**6, bytes_accessed=4 * 10**6, transcendentals=0),
    )(*results)


def solution(mesh):
    placed = (
        P("sp", None),
        P(None, "tp"),
        P("sp", "tp"),
        P("sp", "tp"),
        P("sp", "tp"),
        P("tp", "sp"),
        P("sp", "tp"),
        P("tp"),
        P(),
    )
    return jax.shard_map(
        functools.partial(on_device, mesh.shape["sp"], mesh.shape["tp"]),
        mesh=mesh,
        in_specs=placed,
        out_specs=(P("sp", "tp"), P("sp", "tp"), P("sp", "tp"), P("sp", "tp")),
        check_vma=False,
    )
```

time: 93.3 us -> 96 us (1.029)
  the two profiles are of different devices: /device:TPU:25 before, /device:TPU:1 now
where the time goes in v1:
time: 96 us; the launch traced here: 95.8 us
  Pallas kernels  95.2 us (99%)
    pallas_call x1, Pallas kernels, on_device(): pl.pallas_call(functools.partial(attend_kernel, n, tp_count, heads), out_...  92.8 us
    pallas_call x1, Pallas kernels, on_device(): pl.pallas_call(write_kernel, out_shape=tuple((jax.ShapeDtypeStruct(r.shap...  2.38 us

profile of v1, /device:TPU:1, one launch (start us, length us, event | category | flops | bytes accessed | tf_op | source)
XLA Modules:
  0.0 95.8 jit_solution(7238034008281372420)
XLA Ops:
  0.6 92.8 %shard_map.120 = (bf16[256,1024]{1,0:T(8,128)(2,1)}, bf16[256,256]{1,0:T(8,128)(2,1)}, bf16[256,256]{1,0:T(8,128)(2,1)}, f32[512,256]{1,0:T(8,128)}) custom-call(bf16[256,4096]{1,0:T(8,128)(2,1)} %hidden_ref.1, bf16[4096,256]{1,0:T(8,128)(2,1)} %weight_ref.1, bf16[256,256]{1,0:T(8,128)(2,1)} %values_ref.1, bf16[256,1024]{1,0:T(8,128)(2,1)} %q_in_ref.1, ...), custom_call_target="tpu_custom_call" | custom-call | flops 5000000000 | bytes 10000000 | tf_op jit(solution)/shard_map/pallas_call | solution.py:646
  93.5 2.4 %shard_map.121 = (bf16[256,1024]{1,0:T(8,128)(2,1)}, bf16[256,256]{1,0:T(8,128)(2,1)}, bf16[256,256]{1,0:T(8,128)(2,1)}, f32[512,256]{1,0:T(8,128)}) custom-call(bf16[256,1024]{1,0:T(8,128)(2,1)} %get-tuple-element.8.refs_0_, bf16[256,256]{1,0:T(8,128)(2,1)} %get-tuple-element.9.refs_1_, bf16[256,256]{1,0:T(8,128)(2,1)} %get-tuple-element.10.refs_2_, ...), custom_call_target="tpu_custom_call" | custom-call | flops 1000000 | bytes 4000000 | tf_op jit(solution)/shard_map/pallas_call | solution.py:662

commit v2 on v1

--- a/solution.py
+++ b/solution.py
@@ -104,7 +104,7 @@
     load_sem, q_send, q_recv, d_send, d_recv, m_send, m_recv,
     kv_recv, kv_own, kv_up, kv_pair, p_send, p_recv, dn_send, up_recv,
     gk_recv, gk_up, gk_dn, gk_pair, gk_cross, gv_send, gv_recv, gq_send, gq_recv,
-    hid_send, hid_recv, hid_pass, hid_pair,
+    hid_send, hid_src, hid_recv, hid_pass, hid_pair,
 ):
     me = lax.axis_index("sp")
     tp = lax.axis_index("tp")
@@ -146,7 +146,7 @@
         }[k]
         return pltpu.make_async_copy(src, dst, load_sem.at[k])
 
-    for k in (2, 3, 4, 0, 1, 5, 6):
+    for k in (2, 0, 1, 3, 4, 5, 6):
         load(k).start()
 
     barrier = pltpu.get_barrier_semaphore()
@@ -209,59 +209,74 @@
         return pl.ds(pl.multiple_of(dest * wide, wide), wide)
 
     def hid_slice(dest):
-        return remote(hid_vm.at[own_rows, columns(dest)], hid.at[tp, me], hid_send, hid_recv.at[tp], dest)
-
-    def hid_early():
-        @pl.loop(0, o)
+        return remote(hid_vm.at[own_rows, columns(dest)], hid.at[tp, me], hid_send, hid_src.at[me], dest)
+
+    def hid_down(first, last, side):
+        @pl.loop(first, last)
         def _(l):
-            hid_slice(2 * l + y).start()
-
-    def hid_late():
-        @pl.loop(1, n)
-        def _(k):
-            dest = (me + k) % n
-
-            @pl.when((dest // 2 >= o) | (dest % 2 != y))
+            hid_slice(2 * l + side).start()
+
+    def hid_over(k, b):
+        block = hid.at[tp, b]
+        return remote(block, block, hid_pass.at[k], hid_recv.at[tp], me, (tp + 2 * k) % tp_count)
+
+    def hid_cross(first, last, side):
+        @pl.loop(first, last)
+        def _(l):
+            b = 2 * l + side
+
+            @pl.when(b != me)
             def _():
-                hid_slice(dest).start()
-
-    def hid_wait(sem):
-        pieces = hid.at[tp, pl.ds(0, n - 1)]
-        pltpu.make_async_copy(pieces, pieces, sem).wait()
-
-    def hid_over(k):
-        return remote(hid.at[tp], hid.at[tp], hid_pass.at[k], hid_recv.at[tp], me, (tp + 2 * k) % tp_count)
+                landed(hid.at[tp, b], hid_src.at[b])
+
+            @pl.loop(1, tp_count // 2)
+            def _(k):
+                hid_over(k, b).start()
 
     def hid_to_pair(k):
         source = (tp + 2 * k) % tp_count
         return remote(hid.at[source], hid.at[source], hid_pair.at[k], hid_recv.at[source], me, pair)
 
+    defer = ~home & ~has_up
     load(2).wait()
-    own_copy(1).start()
+
+    @pl.when(~defer)
+    def _():
+        own_copy(1).start()
 
     @pl.when(home & (c == 1) & has_up)
     def _():
         up_copy(me).start()
 
-    for p in range(2):
+    def send_q(p):
         load(p).wait()
 
-    def send_q(p):
         @pl.when(not_self(p))
         def _():
             spread(qb, p, q_send, q_recv).start()
 
-    send_q(0)
+    @pl.when(~has_up)
+    def _():
+        send_q(0)
+        send_q(1)
+
     load(3).wait()
     load(4).wait()
     kv[own_kv, 0] = dot_nn(hid_vm[...], w_vm[...]).astype(jnp.bfloat16)
-    own_copy(0).start()
+
+    @pl.when(~defer)
+    def _():
+        own_copy(0).start()
 
     @pl.when(home & (c == 0) & has_up)
     def _():
         up_copy(me).start()
 
-    send_q(1)
+    @pl.when(has_up)
+    def _():
+        send_q(0)
+        send_q(1)
+
     load(5).wait()
     load(6).wait()
 
@@ -275,8 +290,18 @@
             spread(db, p, d_send, d_recv).start()
             spread(mb, p, m_send, m_recv).start()
 
+    @pl.when(defer)
+    def _():
+        own_copy(1).start()
+        own_copy(0).start()
+
     hid[tp, me] = hid_vm[own_rows, columns(me)]
-    hid_early()
+    hid_down(0, o, y)
+
+    @pl.when(~home)
+    def _():
+        hid_down(0, o + 1, 1 - y)
+
     gw_out[...] = jnp.zeros_like(gw_out)
     gq_t[...] = jnp.zeros_like(gq_t)
 
@@ -365,6 +390,7 @@
                 if part == 0:
                     gkb[b, carried] = (total * SCALE).astype(jnp.bfloat16)
                     gk_up_hop(b, start)
+
                     gk_dn_hop(b, start)
                     gk_deliver(b, start)
                 else:
@@ -387,54 +413,74 @@
         kv_wait(me, 1 - c)
 
     hold(y, grads(me, [y], True), False)
-    take(mate)
-
-    @pl.when(o > 0)
-    def _():
-        @pl.loop(0, 2)
-        def _(j):
-            b = 2 * (o - 1) + jnp.where(j == 0, y, 1 - y)
-            take(b)
-            kv_wait(b, 1 - c)
-            hold(2 + b % 2, grads(b, [y]), False)
+
+    @pl.when(has_up)
+    def _():
+        take(mate)
+
+    count = 2 * o
+
+    def lower(i):
+        return 2 * (o - 1 - i // 2) + jnp.where(i % 2 == 0, y, 1 - y)
+
+    def take_lower(i):
+        @pl.when(i < count)
+        def _():
+            take(lower(i))
+
+    def top_reduce(i):
+        @pl.when(~has_up)
+        def _():
+            reduce(lower(i))
+
+    @pl.loop(0, jnp.minimum(count, 2))
+    def _(i):
+        b = lower(i)
+        take(b)
+        kv_wait(b, 1 - c)
+        hold(2 + i, grads(b, [y]), False)
+
+    take_lower(2)
+    rows_arrive(1 - y)
+
+    @pl.when(home)
+    def _():
+        hid_down(0, o + 1, 1 - y)
+
+    @pl.loop(0, jnp.minimum(count, 2))
+    def _(i):
+        b = lower(i)
+        hold(2 + i, grads(b, [1 - y]), True)
+        emit(b, held(2 + i))
+
+        @pl.when(i == 0)
+        def _():
+            take_lower(3)
+
+            @pl.when(~has_up)
+            def _():
+                take(mate)
+
+        @pl.when(i == 1)
+        def _():
+            top_reduce(0)
+
+    @pl.loop(2, count)
+    def _(i):
+        b = lower(i)
+        kv_wait(b, 1 - c)
+        emit(b, grads(b, [0, 1]))
+        take_lower(i + 2)
+        top_reduce(i - 1)
 
     kv_wait(mate, 1 - c)
-    rows_arrive(1 - y)
     hold(1 - y, grads(mate, [1 - y], True), False)
+    top_reduce(count - 1)
     hold(0, grads(2 * o, [1]), True)
     emit(2 * o, held(0))
     emit(2 * o + 1, held(1))
-
-    @pl.when(o > 0)
-    def _():
-        @pl.loop(0, 2)
-        def _(j):
-            b = 2 * (o - 1) + jnp.where(j == 0, y, 1 - y)
-            hold(2 + b % 2, grads(b, [1 - y]), True)
-            emit(b, held(2 + b % 2))
-
-            @pl.when((j == 0) & ~has_up)
-            def _():
-                each_of(o, reduce)
-
-    @pl.loop(2, o + 1)
-    def _(t):
-        @pl.loop(0, 2)
-        def _(j):
-            b = 2 * (o - t) + jnp.where(j == 0, y, 1 - y)
-            take(b)
-            kv_wait(b, 1 - c)
-            emit(b, grads(b, [0, 1]))
-
-            @pl.when((j == 0) & ~has_up)
-            def _():
-                each_of(o - t + 1, reduce)
-
-    @pl.when(~has_up)
-    def _():
-        each_of(0, reduce)
-
-    hid_late()
+    hid_down(o + 1, outer, y)
+    hid_down(o + 1, outer, 1 - y)
 
     def gq_give(s):
         return remote(gq_fin.at[s], gq_in.at[c], gq_send.at[s], gq_recv.at[c], 2 * o + s, 2 * x + y)
@@ -459,43 +505,40 @@
         def _():
             gq_give(s).start()
 
-    @pl.when(has_up)
-    def _():
-        each_of(o, reduce)
-
-    @pl.loop(o + 1, outer)
-    def _(l):
-        def step(b):
-            landed(gkb.at[b, carried], gk_recv.at[b, carried])
+    near_top = o >= outer - 2
+
+    def hid_relay():
+        hid_to_pair(0).start()
+
+        @pl.loop(1, tp_count // 2)
+        def _(k):
+            source = (tp + 2 * k) % tp_count
+            landed(hid.at[source], hid_recv.at[source])
+            hid_to_pair(k).start()
+
+    def hid_below():
+        hid_cross(0, o, y)
+        hid_cross(0, o, 1 - y)
+
+    hid_cross(o, outer, y)
+    hid_cross(o, outer, 1 - y)
+
+    @pl.when(~near_top)
+    def _():
+        hid_below()
+
+    def gk_step(b):
+        landed(gkb.at[b, carried], gk_recv.at[b, carried])
+
+        @pl.when(b // 2 < o)
+        def _():
+            gk_up_hop(b, start)
+
+        @pl.when(b // 2 > o)
+        def _():
             gk_dn_hop(b, start)
-            gk_deliver(b, start)
-
-        each_of(l, step)
-
-    hid_wait(hid_recv.at[tp])
-
-    @pl.loop(1, tp_count // 2)
-    def _(k):
-        hid_over(k).start()
-
-    hid_to_pair(0).start()
-
-    @pl.when(has_up)
-    def _():
-        @pl.loop(0, o)
-        def _(k):
-            each_of(o - 1 - k, reduce)
-
-    @pl.loop(1, tp_count // 2)
-    def _(k):
-        source = (tp + 2 * k) % tp_count
-        landed(hid.at[source], hid_recv.at[source])
-        hid_to_pair(k).start()
-
-    @pl.loop(0, tp_count // 2)
-    def _(k):
-        source = (pair + 2 * k) % tp_count
-        landed(hid.at[source], hid_recv.at[source])
+
+        gk_deliver(b, start)
 
     def gk_ready(b):
         for h in range(2):
@@ -508,20 +551,72 @@
         block = jnp.concatenate([hid[k, b] for k in range(tp_count)], axis=0)
         gw_out[...] += dot_tn(block, jnp.concatenate([gkb[b, 0], gkb[b, 1]], axis=0))
 
+    def hid_finish():
+        @pl.loop(0, tp_count // 2)
+        def _(k):
+            source = (pair + 2 * k) % tp_count
+            landed(hid.at[source], hid_recv.at[source])
+
+    first_up = jnp.where(near_top, o + 1, o + 2)
+
+    @pl.when(o == 0)
+    def _():
+        hid_relay()
+
+        @pl.loop(1, outer - 1)
+        def _(l):
+            each_of(l, gk_step)
+
+        hid_finish()
+
+        @pl.loop(1, outer - 1)
+        def _(l):
+            each_of(l, add_weight)
+
+    @pl.when((o > 0) & ~near_top)
+    def _():
+        each_of(o + 1, gk_step)
+
+    each_of(o, reduce)
+
+    @pl.when(near_top)
+    def _():
+        hid_below()
+
+    @pl.when(has_up)
+    def _():
+        @pl.loop(0, o)
+        def _(k):
+            each_of(o - 1 - k, reduce)
+
+    @pl.when(o == 1)
+    def _():
+        each_of(0, gk_step)
+
+    @pl.loop(jnp.where(o == 0, outer - 1, first_up), outer)
+    def _(l):
+        each_of(l, gk_step)
+
+    @pl.when(o > 1)
+    def _():
+        each_of(o - 1, gk_step)
+
+    @pl.when(o > 0)
+    def _():
+        hid_relay()
+        hid_finish()
+
     @pl.loop(0, outer)
     def _(k):
         l = jnp.where(k < outer - o, o + k, outer - 1 - k)
 
-        @pl.when(l < o)
-        def _():
-            def step(b):
-                landed(gkb.at[b, carried], gk_recv.at[b, carried])
-                gk_up_hop(b, start)
-                gk_deliver(b, start)
-
-            each_of(l, step)
-
-        each_of(l, add_weight)
+        @pl.when(l < o - 1)
+        def _():
+            each_of(l, gk_step)
+
+        @pl.when((o > 0) | (l == 0) | (l == outer - 1))
+        def _():
+            each_of(l, add_weight)
 
     gk_out[:hrows] = gkb[me, 0]
     gk_out[hrows:] = gkb[me, 1]
@@ -577,11 +672,12 @@
 
         gk_deliver(b, lambda copy: copy.wait_send())
 
-    hid_wait(hid_send)
+    pieces = hid.at[tp, pl.ds(0, n - 1)]
+    landed(pieces, hid_send)
 
     @pl.loop(1, tp_count // 2)
     def _(k):
-        hid_over(k).wait_send()
+        landed(hid.at[tp], hid_pass.at[k])
 
     @pl.loop(0, tp_count // 2)
     def _(k):
@@ -641,6 +737,7 @@
         *[DMA((n,))] * 4,
         *[DMA((2,))] * 4,
         DMA,
+        DMA((n,)),
         *[DMA((tp_count,))] * 3,
     ]
     results = pl.pallas_call(

time: 96 us -> 71.3 us (0.74)
  the two profiles are of different devices: /device:TPU:1 before, /device:TPU:25 now
where the time goes in v2:
time: 71.3 us; the launch traced here: 71.1 us
  Pallas kernels  70.5 us (99%)
    pallas_call x1, Pallas kernels, on_device(): pl.pallas_call(functools.partial(attend_kernel, n, tp_count, heads), out_...  68.1 us
    pallas_call x1, Pallas kernels, on_device(): pl.pallas_call(write_kernel, out_shape=tuple((jax.ShapeDtypeStruct(r.shap...  2.38 us

profile of v2, /device:TPU:25, one launch (start us, length us, event | category | flops | bytes accessed | tf_op | source)
XLA Modules:
  0.0 71.1 jit_solution(15081655069471986855)
XLA Ops:
  0.6 68.1 %shard_map.120 = (bf16[256,1024]{1,0:T(8,128)(2,1)}, bf16[256,256]{1,0:T(8,128)(2,1)}, bf16[256,256]{1,0:T(8,128)(2,1)}, f32[512,256]{1,0:T(8,128)}) custom-call(bf16[256,4096]{1,0:T(8,128)(2,1)} %hidden_ref.1, bf16[4096,256]{1,0:T(8,128)(2,1)} %weight_ref.1, bf16[256,256]{1,0:T(8,128)(2,1)} %values_ref.1, bf16[256,1024]{1,0:T(8,128)(2,1)} %q_in_ref.1, ...), custom_call_target="tpu_custom_call" | custom-call | flops 5000000000 | bytes 10000000 | tf_op jit(solution)/shard_map/pallas_call | solution.py:743
  68.7 2.4 %shard_map.121 = (bf16[256,1024]{1,0:T(8,128)(2,1)}, bf16[256,256]{1,0:T(8,128)(2,1)}, bf16[256,256]{1,0:T(8,128)(2,1)}, f32[512,256]{1,0:T(8,128)}) custom-call(bf16[256,1024]{1,0:T(8,128)(2,1)} %get-tuple-element.8.refs_0_, bf16[256,256]{1,0:T(8,128)(2,1)} %get-tuple-element.9.refs_1_, bf16[256,256]{1,0:T(8,128)(2,1)} %get-tuple-element.10.refs_2_, ...), custom_call_target="tpu_custom_call" | custom-call | flops 1000000 | bytes 4000000 | tf_op jit(solution)/shard_map/pallas_call | solution.py:759

commit v3 on v2

--- a/solution.py
+++ b/solution.py
@@ -114,6 +114,7 @@
     x, c = tp // 2, tp % 2
     mate, pair = me + 1 - 2 * y, tp + 1 - 2 * c
     has_up = o < outer - 1
+    near_top = o >= outer - 2
     home = y == c
     rows = og_in_ref.shape[0]
     hrows = rows // 2
@@ -183,10 +184,10 @@
         )
 
     def up_copy(b):
-        return remote(kv.at[b, c], kv.at[b, c], kv_up.at[b], kv_recv.at[b, c], me + 2)
+        return remote(kv.at[b, c], kv.at[b, c], kv_up, kv_recv.at[b, c], me + 2)
 
     def pair_copy(b):
-        return remote(kv.at[b, c], kv.at[b, c], kv_pair.at[b], kv_recv.at[b, c], me, pair)
+        return remote(kv.at[b, c], kv.at[b, c], kv_pair, kv_recv.at[b, c], me, pair)
 
     def kv_wait(b, p):
         landed(kv.at[b, p], kv_recv.at[b, p])
@@ -318,7 +319,7 @@
                 acc[at, part, :, cols] = piece
 
     def partial(b):
-        return remote(p_out.at[b], p_in.at[b], p_send.at[b], p_recv.at[b], me, pair)
+        return remote(p_out.at[b], p_in.at[b], p_send, p_recv.at[b], me, pair)
 
     def emit(b, pieces):
         for part, col, piece in pieces:
@@ -332,15 +333,16 @@
         return [(part, 0, acc[at, part]) for part in range(2)]
 
     carried = jnp.where(home, c, 2)
+    reach = 3
 
     def down(b, part):
-        return remote(dn_out.at[b, part], up_in.at[b, part], dn_send.at[b, part], up_recv.at[b, part], me - 2)
+        return remote(dn_out.at[b, part], up_in.at[b, part], dn_send, up_recv.at[b, part], me - 2)
 
     def gk_hop(b, sems, target):
-        return remote(gkb.at[b, carried], gkb.at[b, carried], sems.at[b], gk_recv.at[b, carried], target)
+        return remote(gkb.at[b, carried], gkb.at[b, carried], sems, gk_recv.at[b, 1], target)
 
     def gk_give(b, sems, target, to):
-        return remote(gkb.at[b, carried], gkb.at[b, c], sems.at[b], gk_recv.at[b, c], target, to)
+        return remote(gkb.at[b, carried], gkb.at[b, c], sems, gk_recv.at[b, 0], target, to)
 
     def gk_deliver(b, act):
         act(gk_give(b, gk_cross, mate, 2 * x + y))
@@ -350,9 +352,12 @@
             act(gk_give(b, gk_pair, me, pair))
 
     def gk_up_hop(b, act):
-        @pl.when(has_up)
-        def _():
-            act(gk_hop(b, gk_up, me + 2))
+        @pl.when((o - b // 2) % reach == 0)
+        def _():
+            for k in range(reach, 0, -1):
+                @pl.when(o + k < outer)
+                def _():
+                    act(gk_hop(b, gk_up, me + 2 * k))
 
     def gk_dn_hop(b, act):
         @pl.when(o > 0)
@@ -370,40 +375,43 @@
         def _(j):
             act(2 * level + jnp.where(j == 0, y, 1 - y))
 
-    def reduce(b):
-        landed(p_in.at[b], p_recv.at[b])
-        for part in range(2):
-            @pl.when(has_up)
-            def _():
-                landed(up_in.at[b, part], up_recv.at[b, part])
-                keep[b, part] += up_in[b, part].astype(jnp.float32)
-
-            total = keep[b, part] + p_in[b, part].astype(jnp.float32)
-
-            @pl.when(b // 2 < o)
-            def _():
-                dn_out[b, part] = total.astype(jnp.bfloat16)
-                down(b, part).start()
-
-            @pl.when(b // 2 == o)
-            def _():
-                if part == 0:
-                    gkb[b, carried] = (total * SCALE).astype(jnp.bfloat16)
-                    gk_up_hop(b, start)
-
-                    gk_dn_hop(b, start)
-                    gk_deliver(b, start)
-                else:
-                    s = b % 2
-
-                    @pl.when(home & (s == y))
-                    def _():
-                        gv_in[c] = total.astype(jnp.bfloat16)
-
-                    @pl.when(~(home & (s == y)))
-                    def _():
-                        gv_fin[s] = total.astype(jnp.bfloat16)
-                        gv_give(s).start()
+    def reduce(b, part):
+        if part == 0:
+            landed(p_in.at[b], p_recv.at[b])
+
+        @pl.when(has_up)
+        def _():
+            landed(up_in.at[b, part], up_recv.at[b, part])
+            keep[b, part] += up_in[b, part].astype(jnp.float32)
+
+        total = keep[b, part] + p_in[b, part].astype(jnp.float32)
+
+        @pl.when(b // 2 < o)
+        def _():
+            dn_out[b, part] = total.astype(jnp.bfloat16)
+            down(b, part).start()
+
+        @pl.when(b // 2 == o)
+        def _():
+            if part == 0:
+                gkb[b, carried] = (total * SCALE).astype(jnp.bfloat16)
+                gk_up_hop(b, start)
+                gk_dn_hop(b, start)
+                gk_deliver(b, start)
+            else:
+                s = b % 2
+
+                @pl.when(home & (s == y))
+                def _():
+                    gv_in[c] = total.astype(jnp.bfloat16)
+
+                @pl.when(~(home & (s == y)))
+                def _():
+                    gv_fin[s] = total.astype(jnp.bfloat16)
+                    gv_give(s).start()
+
+    def sums(level, part):
+        each_of(level, lambda b: reduce(b, part))
 
     @pl.when(~home)
     def _():
@@ -431,7 +439,11 @@
     def top_reduce(i):
         @pl.when(~has_up)
         def _():
-            reduce(lower(i))
+            reduce(lower(i), 0)
+
+            @pl.when(i < 2)
+            def _():
+                reduce(lower(i), 1)
 
     @pl.loop(0, jnp.minimum(count, 2))
     def _(i):
@@ -441,6 +453,11 @@
         hold(2 + i, grads(b, [y]), False)
 
     take_lower(2)
+
+    @pl.when(has_up)
+    def _():
+        take_lower(3)
+
     rows_arrive(1 - y)
 
     @pl.when(home)
@@ -453,17 +470,17 @@
         hold(2 + i, grads(b, [1 - y]), True)
         emit(b, held(2 + i))
 
-        @pl.when(i == 0)
+        @pl.when((i == 0) & ~has_up)
         def _():
             take_lower(3)
 
-            @pl.when(~has_up)
-            def _():
-                take(mate)
-
         @pl.when(i == 1)
         def _():
             top_reduce(0)
+
+    hid_down(o + 1, outer, y)
+    hid_down(o + 1, outer, 1 - y)
+    hid_cross(o, outer, y)
 
     @pl.loop(2, count)
     def _(i):
@@ -473,14 +490,27 @@
         take_lower(i + 2)
         top_reduce(i - 1)
 
+    @pl.when(~has_up)
+    def _():
+        take(mate)
+        hid_cross(o, outer, 1 - y)
+        hid_cross(o - 1, o, y)
+        hid_cross(o - 1, o, 1 - y)
+
     kv_wait(mate, 1 - c)
     hold(1 - y, grads(mate, [1 - y], True), False)
     top_reduce(count - 1)
     hold(0, grads(2 * o, [1]), True)
     emit(2 * o, held(0))
     emit(2 * o + 1, held(1))
-    hid_down(o + 1, outer, y)
-    hid_down(o + 1, outer, 1 - y)
+
+    @pl.when(~has_up & (count > 2))
+    def _():
+        sums(0, 1)
+
+    @pl.when(has_up & near_top)
+    def _():
+        hid_cross(o, outer, 1 - y)
 
     def gq_give(s):
         return remote(gq_fin.at[s], gq_in.at[c], gq_send.at[s], gq_recv.at[c], 2 * o + s, 2 * x + y)
@@ -505,8 +535,6 @@
         def _():
             gq_give(s).start()
 
-    near_top = o >= outer - 2
-
     def hid_relay():
         hid_to_pair(0).start()
 
@@ -516,19 +544,17 @@
             landed(hid.at[source], hid_recv.at[source])
             hid_to_pair(k).start()
 
-    def hid_below():
-        hid_cross(0, o, y)
-        hid_cross(0, o, 1 - y)
-
-    hid_cross(o, outer, y)
-    hid_cross(o, outer, 1 - y)
+    def hid_below(last):
+        hid_cross(0, last, y)
+        hid_cross(0, last, 1 - y)
 
     @pl.when(~near_top)
     def _():
-        hid_below()
+        hid_cross(o, outer, 1 - y)
+        hid_below(o)
 
     def gk_step(b):
-        landed(gkb.at[b, carried], gk_recv.at[b, carried])
+        landed(gkb.at[b, carried], gk_recv.at[b, 1])
 
         @pl.when(b // 2 < o)
         def _():
@@ -541,10 +567,13 @@
         gk_deliver(b, start)
 
     def gk_ready(b):
-        for h in range(2):
-            @pl.when(~(home & (c == h)))
-            def _():
-                landed(gkb.at[b, h], gk_recv.at[b, h])
+        @pl.when(home)
+        def _():
+            landed(gkb.at[b, 0], gk_recv.at[b, 0])
+
+        @pl.when(~home)
+        def _():
+            landed(gkb.at[b, pl.ds(0, 2)], gk_recv.at[b, 0])
 
     def add_weight(b):
         gk_ready(b)
@@ -557,6 +586,64 @@
             source = (pair + 2 * k) % tp_count
             landed(hid.at[source], hid_recv.at[source])
 
+    def settle():
+        for p in range(2):
+            own_copy(p).wait_send()
+
+            @pl.when(not_self(p))
+            def _():
+                spread(qb, p, q_send, q_recv).wait_send()
+                spread(db, p, d_send, d_recv).wait_send()
+                spread(mb, p, m_send, m_recv).wait_send()
+
+            @pl.when(~(home & (y == p)))
+            def _():
+                gq_give(p).wait_send()
+
+            @pl.when(~(home & (c == p)))
+            def _():
+                landed(gq_in.at[p], gq_recv.at[p])
+
+            gq_out[:, p * pair_q : (p + 1) * pair_q] = gq_in[p]
+
+        for l in range(outer):
+            @pl.when(o == l)
+            def _():
+                if l < outer - 1:
+                    landed(kv.at[pl.ds(0, 2 * l + 2), 0], kv_up)
+                landed(kv.at[pl.ds(0, 2 * l + 1), 0], kv_pair)
+                landed(p_out.at[pl.ds(0, 2 * l + 2)], p_send)
+
+        landed(hid.at[tp, pl.ds(0, n - 1)], hid_send)
+
+        @pl.loop(1, tp_count // 2)
+        def _(k):
+            landed(hid.at[tp], hid_pass.at[k])
+
+    def finish():
+        gk_out[:hrows] = gkb[me, 0]
+        gk_out[hrows:] = gkb[me, 1]
+        for h in range(2):
+            @pl.when(~(home & (c == h)))
+            def _():
+                landed(gv_in.at[h], gv_recv.at[h])
+
+            gv_out[h * hrows : (h + 1) * hrows] = gv_in[h]
+
+            @pl.when(~(home & (y == h)))
+            def _():
+                gv_give(h).wait_send()
+
+        for l in range(1, outer):
+            @pl.when(o == l)
+            def _():
+                landed(dn_out.at[pl.ds(0, 2 * l)], dn_send)
+                landed(gkb.at[pl.ds(0, n - 2 * l), 0], gk_dn)
+
+        @pl.loop(0, tp_count // 2)
+        def _(k):
+            hid_to_pair(k).wait_send()
+
     first_up = jnp.where(near_top, o + 1, o + 2)
 
     @pl.when(o == 0)
@@ -573,120 +660,85 @@
         def _(l):
             each_of(l, add_weight)
 
+        settle()
+
     @pl.when((o > 0) & ~near_top)
     def _():
         each_of(o + 1, gk_step)
 
-    each_of(o, reduce)
+    sums(o, 0)
+
+    @pl.when((o == outer - 2) | (o == 0))
+    def _():
+        sums(o, 1)
 
     @pl.when(near_top)
     def _():
-        hid_below()
-
-    @pl.when(has_up)
+        hid_below(jnp.where(has_up, o, o - 1))
+
+    @pl.when(has_up & (o > 0))
     def _():
         @pl.loop(0, o)
         def _(k):
-            each_of(o - 1 - k, reduce)
-
-    @pl.when(o == 1)
-    def _():
-        each_of(0, gk_step)
+            sums(o - 1 - k, 0)
+
+        sums(0, 1)
 
     @pl.loop(jnp.where(o == 0, outer - 1, first_up), outer)
     def _(l):
         each_of(l, gk_step)
 
-    @pl.when(o > 1)
-    def _():
-        each_of(o - 1, gk_step)
+    @pl.loop(1, jnp.where(has_up, o, o - 1))
+    def _(l):
+        sums(l, 1)
+
+    @pl.when((o != outer - 2) & (o > 0))
+    def _():
+        sums(o, 1)
+
+    @pl.loop(1, o)
+    def _(k):
+        each_of(o - k, gk_step)
 
     @pl.when(o > 0)
     def _():
         hid_relay()
         hid_finish()
+        settle()
+        each_of(0, gk_step)
 
     @pl.loop(0, outer)
     def _(k):
         l = jnp.where(k < outer - o, o + k, outer - 1 - k)
 
-        @pl.when(l < o - 1)
-        def _():
-            each_of(l, gk_step)
+        @pl.when(k == outer - 1)
+        def _():
+            finish()
 
         @pl.when((o > 0) | (l == 0) | (l == outer - 1))
         def _():
             each_of(l, add_weight)
 
-    gk_out[:hrows] = gkb[me, 0]
-    gk_out[hrows:] = gkb[me, 1]
-    for h in range(2):
-        @pl.when(~(home & (c == h)))
-        def _():
-            landed(gv_in.at[h], gv_recv.at[h])
-            landed(gq_in.at[h], gq_recv.at[h])
-
-        gv_out[h * hrows : (h + 1) * hrows] = gv_in[h]
-        gq_out[:, h * pair_q : (h + 1) * pair_q] = gq_in[h]
-
-    for p in range(2):
-        own_copy(p).wait_send()
-
-        @pl.when(not_self(p))
-        def _():
-            spread(qb, p, q_send, q_recv).wait_send()
-            spread(db, p, d_send, d_recv).wait_send()
-            spread(mb, p, m_send, m_recv).wait_send()
-
-        @pl.when(~(home & (y == p)))
-        def _():
-            gv_give(p).wait_send()
-            gq_give(p).wait_send()
-
-    @pl.loop(0, 2 * o + 2)
-    def _(b):
-        @pl.when(has_up)
-        def _():
-            up_copy(b).wait_send()
-
-        @pl.when(b != me)
-        def _():
-            pair_copy(b).wait_send()
-
-        partial(b).wait_send()
-
-        @pl.when(b // 2 < o)
-        def _():
-            for part in range(2):
-                down(b, part).wait_send()
-
-    @pl.loop(0, n)
-    def _(b):
-        @pl.when(b // 2 <= o)
-        def _():
-            gk_up_hop(b, lambda copy: copy.wait_send())
-
-        @pl.when(b // 2 >= o)
-        def _():
-            gk_dn_hop(b, lambda copy: copy.wait_send())
-
-        gk_deliver(b, lambda copy: copy.wait_send())
-
-    pieces = hid.at[tp, pl.ds(0, n - 1)]
-    landed(pieces, hid_send)
-
-    @pl.loop(1, tp_count // 2)
-    def _(k):
-        landed(hid.at[tp], hid_pass.at[k])
-
-    @pl.loop(0, tp_count // 2)
-    def _(k):
-        hid_to_pair(k).wait_send()
+    for l in range(outer - 1):
+        hops = 2 * min(reach, outer - 1 - l) * (l // reach + 1)
+
+        @pl.when(o == l)
+        def _():
+            landed(gkb.at[pl.ds(0, hops), 0], gk_up)
+
+    landed(gkb.at[pl.ds(0, n), 0], gk_cross)
+
+    @pl.when(~home)
+    def _():
+        landed(gkb.at[pl.ds(0, n), 0], gk_pair)
 
 
 def write_kernel(*refs):
-    for src, dst in zip(refs[:4], refs[4:]):
-        dst[...] = src[...]
+    copies = [pltpu.make_async_copy(refs[k], refs[4 + k], refs[8].at[k]) for k in range(4)]
+    for copy in copies:
+        copy.start()
+    for copy in copies:
+        copy.wait()
 
 
 def on_device(n, tp_count, hidden, key_weight, queries, values, map_out, log_sums, out_grad, mixing, out_gain):
@@ -727,26 +779,25 @@
         *[DMA((2,))] * 6,
         DMA((n, 2)),
         DMA((2,)),
+        *[DMA] * 3,
         DMA((n,)),
-        DMA((n,)),
-        DMA((n,)),
-        DMA((n,)),
+        DMA,
         DMA((n, 2)),
         DMA((n, 2)),
-        DMA((n, 3)),
-        *[DMA((n,))] * 4,
+        *[DMA] * 4,
         *[DMA((2,))] * 4,
         DMA,
         DMA((n,)),
-        *[DMA((tp_count,))] * 3,
+        DMA((tp_count,)),
+        *[DMA((tp_count // 2,))] * 2,
     ]
     results = pl.pallas_call(
         functools.partial(attend_kernel, n, tp_count, heads),
         out_shape=(
-            jax.ShapeDtypeStruct(queries.shape, bf16),
-            jax.ShapeDtypeStruct((rows, width), bf16),
-            jax.ShapeDtypeStruct((rows, width), bf16),
-            jax.ShapeDtypeStruct((hidden.shape[1] // n, width), f32),
+            VMEM(queries.shape, bf16),
+            VMEM((rows, width), bf16),
+            VMEM((rows, width), bf16),
+            VMEM((hidden.shape[1] // n, width), f32),
         ),
         in_specs=[hbm] * 6 + [vm] * 2 + [pl.BlockSpec(memory_space=pltpu.SMEM)],
         out_specs=(vm, vm, vm, vm),
@@ -760,9 +811,10 @@
         write_kernel,
         out_shape=tuple(jax.ShapeDtypeStruct(r.shape, r.dtype) for r in results),
         in_specs=[vm] * 4,
-        out_specs=(vm,) * 4,
+        out_specs=(hbm,) * 4,
+        scratch_shapes=[DMA((4,))],
         cost_estimate=pl.CostEstimate(flops=10**6, bytes_accessed=4 * 10**6, transcendentals=0),
-    )(*results)
+    )(*[pltpu.with_memory_space_constraint(r, VMEM) for r in results])
 
 
 def solution(mesh):

time: 71.3 us -> 62.6 us (0.88)
  the two profiles are of different devices: /device:TPU:25 before, /device:TPU:9 now
where the time goes in v3:
time: 62.6 us; the launch traced here: 62.4 us
  Pallas kernels  61.7 us (99%)
  between operations  0.64 us (1%)
    pallas_call x1, Pallas kernels, on_device(): pl.pallas_call(functools.partial(attend_kernel, n, tp_count, heads), out_...  60.6 us

profile of v3, /device:TPU:9, one launch (start us, length us, event | category | flops | bytes accessed | tf_op | source)
XLA Modules:
  0.0 62.4 jit_solution(1262248145324477110)
XLA Ops:
  0.6 60.6 %shard_map.120 = (bf16[256,1024]{1,0:T(8,128)(2,1)S(1)}, bf16[256,256]{1,0:T(8,128)(2,1)S(1)}, bf16[256,256]{1,0:T(8,128)(2,1)S(1)}, f32[512,256]{1,0:T(8,128)S(1)}) custom-call(bf16[256,4096]{1,0:T(8,128)(2,1)} %hidden_ref.1, bf16[4096,256]{1,0:T(8,128)(2,1)} %weight_ref.1, bf16[256,256]{1,0:T(8,128)(2,1)} %values_ref.1, bf16[256,1024]{1,0:T(8,128)(2,1)} %q_in_ref.1, ...), custom_call_target="tpu_custom_call" | custom-call | flops 5000000000 | bytes 10000000 | tf_op jit(solution)/shard_map/pallas_call | solution.py:794
  61.3 1.1 %shard_map.121 = (bf16[256,1024]{1,0:T(8,128)(2,1)}, bf16[256,256]{1,0:T(8,128)(2,1)}, bf16[256,256]{1,0:T(8,128)(2,1)}, f32[512,256]{1,0:T(8,128)}) custom-call(bf16[256,1024]{1,0:T(8,128)(2,1)S(1)} %get-tuple-element.8.refs_0_, bf16[256,256]{1,0:T(8,128)(2,1)S(1)} %get-tuple-element.9.refs_1_, bf16[256,256]{1,0:T(8,128)(2,1)S(1)} %get-tuple-element.10.refs_2_, ...), custom_call_target="tpu_custom_call" | custom-call | flops 1000000 | bytes 4000000 | tf_op jit(solution)/shard_map/pallas_call | solution.py:810

commit v4 on v3

--- a/solution.py
+++ b/solution.py
@@ -351,13 +351,23 @@
         def _():
             act(gk_give(b, gk_pair, me, pair))
 
-    def gk_up_hop(b, act):
-        @pl.when((o - b // 2) % reach == 0)
-        def _():
-            for k in range(reach, 0, -1):
-                @pl.when(o + k < outer)
-                def _():
-                    act(gk_hop(b, gk_up, me + 2 * k))
+    def gk_up_near(b):
+        dist = (o - b // 2) % reach
+
+        @pl.when(has_up & ((dist == 0) | ((dist == 1) & (o + 2 < outer))))
+        def _():
+            gk_hop(b, gk_up, me + 2).start()
+
+    def gk_up_far(b):
+        root = (o - b // 2) % reach == 0
+
+        @pl.when(root & (o + 3 < outer))
+        def _():
+            gk_hop(b, gk_up, me + 6).start()
+
+        @pl.when(root & (o + 3 == outer))
+        def _():
+            gk_hop(b, gk_up, me + 4).start()
 
     def gk_dn_hop(b, act):
         @pl.when(o > 0)
@@ -395,7 +405,12 @@
         def _():
             if part == 0:
                 gkb[b, carried] = (total * SCALE).astype(jnp.bfloat16)
-                gk_up_hop(b, start)
+                gk_up_near(b)
+
+                @pl.when(b % 2 != y)
+                def _():
+                    each_of(o, gk_up_far)
+
                 gk_dn_hop(b, start)
                 gk_deliver(b, start)
             else:
@@ -441,76 +456,105 @@
         def _():
             reduce(lower(i), 0)
 
-            @pl.when(i < 2)
-            def _():
-                reduce(lower(i), 1)
-
-    @pl.loop(0, jnp.minimum(count, 2))
+            @pl.when(i == 1)
+            def _():
+                reduce(lower(0), 1)
+                reduce(lower(1), 1)
+
+    ahead = jnp.minimum(count, jnp.where(has_up, 4, 2))
+
+    @pl.loop(0, ahead)
     def _(i):
         b = lower(i)
         take(b)
         kv_wait(b, 1 - c)
         hold(2 + i, grads(b, [y]), False)
 
-    take_lower(2)
+    @pl.when(~has_up)
+    def _():
+        take_lower(2)
+
+    rows_arrive(1 - y)
+
+    @pl.when(home)
+    def _():
+        hid_down(0, o + 1, 1 - y)
+
+    def own_level():
+        kv_wait(mate, 1 - c)
+        hold(1 - y, grads(mate, [1 - y], True), False)
+        top_reduce(count - 1)
+        hold(0, grads(2 * o, [1]), True)
+        emit(2 * o, held(0))
+        emit(2 * o + 1, held(1))
+
+    def hid_up():
+        hid_down(o + 1, outer, y)
+        hid_down(o + 1, outer, 1 - y)
+
+    @pl.when(o == 0)
+    def _():
+        hid_up()
 
     @pl.when(has_up)
     def _():
-        take_lower(3)
-
-    rows_arrive(1 - y)
-
-    @pl.when(home)
-    def _():
-        hid_down(0, o + 1, 1 - y)
-
-    @pl.loop(0, jnp.minimum(count, 2))
+        own_level()
+
+    @pl.when(o > 0)
+    def _():
+        hid_up()
+
+    below_top = has_up & near_top
+
+    @pl.loop(0, ahead)
     def _(i):
         b = lower(i)
         hold(2 + i, grads(b, [1 - y]), True)
         emit(b, held(2 + i))
 
-        @pl.when((i == 0) & ~has_up)
-        def _():
-            take_lower(3)
-
         @pl.when(i == 1)
         def _():
             top_reduce(0)
 
-    hid_down(o + 1, outer, y)
-    hid_down(o + 1, outer, 1 - y)
+            @pl.when(below_top)
+            def _():
+                sums(o, 0)
+
     hid_cross(o, outer, y)
 
-    @pl.loop(2, count)
+    @pl.when(has_up)
+    def _():
+        take_lower(4)
+        take_lower(5)
+
+    @pl.loop(ahead, count)
     def _(i):
         b = lower(i)
         kv_wait(b, 1 - c)
         emit(b, grads(b, [0, 1]))
+        top_reduce(i - 1)
+
+        @pl.when((i == 2) & ~has_up)
+        def _():
+            take_lower(3)
+
         take_lower(i + 2)
-        top_reduce(i - 1)
+
+        @pl.when((i == count - 2) & ~has_up)
+        def _():
+            take(mate)
 
     @pl.when(~has_up)
     def _():
-        take(mate)
-        hid_cross(o, outer, 1 - y)
-        hid_cross(o - 1, o, y)
-        hid_cross(o - 1, o, 1 - y)
-
-    kv_wait(mate, 1 - c)
-    hold(1 - y, grads(mate, [1 - y], True), False)
-    top_reduce(count - 1)
-    hold(0, grads(2 * o, [1]), True)
-    emit(2 * o, held(0))
-    emit(2 * o + 1, held(1))
-
-    @pl.when(~has_up & (count > 2))
-    def _():
-        sums(0, 1)
-
-    @pl.when(has_up & near_top)
-    def _():
-        hid_cross(o, outer, 1 - y)
+        @pl.when(count == 2)
+        def _():
+            take(mate)
+
+        own_level()
+
+        @pl.when(count > 2)
+        def _():
+            sums(0, 1)
 
     def gq_give(s):
         return remote(gq_fin.at[s], gq_in.at[c], gq_send.at[s], gq_recv.at[c], 2 * o + s, 2 * x + y)
@@ -558,7 +602,8 @@
 
         @pl.when(b // 2 < o)
         def _():
-            gk_up_hop(b, start)
+            gk_up_near(b)
+            gk_up_far(b)
 
         @pl.when(b // 2 > o)
         def _():
@@ -655,26 +700,31 @@
             each_of(l, gk_step)
 
         hid_finish()
-
+        settle()
+
+    @pl.when((o > 0) & ~near_top)
+    def _():
+        each_of(o + 1, gk_step)
+
+    @pl.when(~below_top)
+    def _():
+        sums(o, 0)
+
+    @pl.when(~has_up)
+    def _():
+        hid_cross(o, outer, 1 - y)
+        hid_cross(o - 1, o, y)
+        hid_cross(o - 1, o, 1 - y)
+
+    @pl.when(o == 0)
+    def _():
         @pl.loop(1, outer - 1)
         def _(l):
             each_of(l, add_weight)
 
-        settle()
-
-    @pl.when((o > 0) & ~near_top)
-    def _():
-        each_of(o + 1, gk_step)
-
-    sums(o, 0)
-
     @pl.when((o == outer - 2) | (o == 0))
     def _():
         sums(o, 1)
-
-    @pl.when(near_top)
-    def _():
-        hid_below(jnp.where(has_up, o, o - 1))
 
     @pl.when(has_up & (o > 0))
     def _():
@@ -682,12 +732,29 @@
         def _(k):
             sums(o - 1 - k, 0)
 
+            @pl.when(near_top & (k == 0))
+            def _():
+                hid_cross(o, outer, 1 - y)
+                hid_below(o)
+
         sums(0, 1)
+
+    @pl.when(~has_up)
+    def _():
+        hid_below(o - 1)
+
+    @pl.when((o == 1) & has_up)
+    def _():
+        hid_relay()
 
     @pl.loop(jnp.where(o == 0, outer - 1, first_up), outer)
     def _(l):
         each_of(l, gk_step)
 
+    @pl.when((o == 1) & has_up)
+    def _():
+        each_of(0, gk_step)
+
     @pl.loop(1, jnp.where(has_up, o, o - 1))
     def _(l):
         sums(l, 1)
@@ -700,27 +767,34 @@
     def _(k):
         each_of(o - k, gk_step)
 
+    @pl.when((o > 1) | ~has_up)
+    def _():
+        hid_relay()
+
     @pl.when(o > 0)
     def _():
-        hid_relay()
         hid_finish()
         settle()
+
+        @pl.loop(1, outer)
+        def _(k):
+            each_of(jnp.where(k < outer - o + 1, o + k - 1, outer - k), add_weight)
+
+    @pl.when(o == 0)
+    def _():
+        each_of(0, add_weight)
+
+    finish()
+
+    @pl.when((o > 1) | ~has_up)
+    def _():
         each_of(0, gk_step)
 
-    @pl.loop(0, outer)
-    def _(k):
-        l = jnp.where(k < outer - o, o + k, outer - 1 - k)
-
-        @pl.when(k == outer - 1)
-        def _():
-            finish()
-
-        @pl.when((o > 0) | (l == 0) | (l == outer - 1))
-        def _():
-            each_of(l, add_weight)
+    each_of(jnp.where(o == 0, outer - 1, 0), add_weight)
 
     for l in range(outer - 1):
-        hops = 2 * min(reach, outer - 1 - l) * (l // reach + 1)
+        roots, nexts = l // reach + 1, (l - 1) // reach + 1
+        hops = 2 * roots * min(2, outer - 1 - l) + 2 * nexts * (l + 2 < outer)
 
         @pl.when(o == l)
         def _():
@@ -760,7 +834,7 @@
         VMEM((4, rows, half * V_DIM), bf16),
         VMEM((4, 4 * half, rows), f32),
         VMEM((n + 1, 2, rows, width), bf16),
-        VMEM((4, 2, rows, width), f32),
+        VMEM((6, 2, rows, width), f32),
         VMEM((n, 2, hrows, width), f32),
         VMEM((n, 2, hrows, width), bf16),
         VMEM((n, 2, hrows, width), bf16),

time: 62.6 us -> 57.2 us (0.914)
  the two profiles are of different devices: /device:TPU:9 before, /device:TPU:25 now
where the time goes in v4:
time: 57.2 us; the launch traced here: 57 us
  Pallas kernels  56.3 us (98%)
  between operations  0.64 us (1%)
    pallas_call x1, Pallas kernels, on_device(): pl.pallas_call(functools.partial(attend_kernel, n, tp_count, heads), out_...  55.2 us

profile of v4, /device:TPU:25, one launch (start us, length us, event | category | flops | bytes accessed | tf_op | source)
XLA Modules:
  0.0 57.0 jit_solution(17262821571013602261)
XLA Ops:
  0.6 55.2 %shard_map.120 = (bf16[256,1024]{1,0:T(8,128)(2,1)S(1)}, bf16[256,256]{1,0:T(8,128)(2,1)S(1)}, bf16[256,256]{1,0:T(8,128)(2,1)S(1)}, f32[512,256]{1,0:T(8,128)S(1)}) custom-call(bf16[256,4096]{1,0:T(8,128)(2,1)} %hidden_ref.1, bf16[4096,256]{1,0:T(8,128)(2,1)} %weight_ref.1, bf16[256,256]{1,0:T(8,128)(2,1)} %values_ref.1, bf16[256,1024]{1,0:T(8,128)(2,1)} %q_in_ref.1, ...), custom_call_target="tpu_custom_call" | custom-call | flops 5000000000 | bytes 10000000 | tf_op jit(solution)/shard_map/pallas_call | solution.py:868
  55.9 1.1 %shard_map.121 = (bf16[256,1024]{1,0:T(8,128)(2,1)}, bf16[256,256]{1,0:T(8,128)(2,1)}, bf16[256,256]{1,0:T(8,128)(2,1)}, f32[512,256]{1,0:T(8,128)}) custom-call(bf16[256,1024]{1,0:T(8,128)(2,1)S(1)} %get-tuple-element.8.refs_0_, bf16[256,256]{1,0:T(8,128)(2,1)S(1)} %get-tuple-element.9.refs_1_, bf16[256,256]{1,0:T(8,128)(2,1)S(1)} %get-tuple-element.10.refs_2_, ...), custom_call_target="tpu_custom_call" | custom-call | flops 1000000 | bytes 4000000 | tf_op jit(solution)/shard_map/pallas_call | solution.py:884

commit v5 on v4

--- a/solution.py
+++ b/solution.py
@@ -732,10 +732,10 @@
         def _(k):
             sums(o - 1 - k, 0)
 
-            @pl.when(near_top & (k == 0))
-            def _():
-                hid_cross(o, outer, 1 - y)
-                hid_below(o)
+        @pl.when(near_top)
+        def _():
+            hid_cross(o, outer, 1 - y)
+            hid_below(o)
 
         sums(0, 1)
 
@@ -776,6 +776,10 @@
         hid_finish()
         settle()
 
+        @pl.when((o > 1) | ~has_up)
+        def _():
+            each_of(0, gk_step)
+
         @pl.loop(1, outer)
         def _(k):
             each_of(jnp.where(k < outer - o + 1, o + k - 1, outer - k), add_weight)
@@ -785,11 +789,6 @@
         each_of(0, add_weight)
 
     finish()
-
-    @pl.when((o > 1) | ~has_up)
-    def _():
-        each_of(0, gk_step)
-
     each_of(jnp.where(o == 0, outer - 1, 0), add_weight)
 
     for l in range(outer - 1):

time: 57.2 us -> 55.8 us (0.976)
  Pallas kernels: 56.3 us -> 54.5 us
    pallas_call x1, Pallas kernels: 55.2 us -> 53.4 us  [on_device(): pl.pallas_call(functools.partial(attend_kernel, n, tp_count, heads), out_...]
where the time goes in v5:
time: 55.8 us; the launch traced here: 55.2 us
  Pallas kernels  54.5 us (98%)
  between operations  0.64 us (1%)
    pallas_call x1, Pallas kernels, on_device(): pl.pallas_call(functools.partial(attend_kernel, n, tp_count, heads), out_...  53.4 us

profile of v5, /device:TPU:25, one launch (start us, length us, event | category | flops | bytes accessed | tf_op | source)
XLA Modules:
  0.0 55.2 jit_solution(603307710220739587)
XLA Ops:
  0.6 53.4 %shard_map.120 = (bf16[256,1024]{1,0:T(8,128)(2,1)S(1)}, bf16[256,256]{1,0:T(8,128)(2,1)S(1)}, bf16[256,256]{1,0:T(8,128)(2,1)S(1)}, f32[512,256]{1,0:T(8,128)S(1)}) custom-call(bf16[256,4096]{1,0:T(8,128)(2,1)} %hidden_ref.1, bf16[4096,256]{1,0:T(8,128)(2,1)} %weight_ref.1, bf16[256,256]{1,0:T(8,128)(2,1)} %values_ref.1, bf16[256,1024]{1,0:T(8,128)(2,1)} %q_in_ref.1, ...), custom_call_target="tpu_custom_call" | custom-call | flops 5000000000 | bytes 10000000 | tf_op jit(solution)/shard_map/pallas_call | solution.py:867
  54.1 1.1 %shard_map.121 = (bf16[256,1024]{1,0:T(8,128)(2,1)}, bf16[256,256]{1,0:T(8,128)(2,1)}, bf16[256,256]{1,0:T(8,128)(2,1)}, f32[512,256]{1,0:T(8,128)}) custom-call(bf16[256,1024]{1,0:T(8,128)(2,1)S(1)} %get-tuple-element.8.refs_0_, bf16[256,256]{1,0:T(8,128)(2,1)S(1)} %get-tuple-element.9.refs_1_, bf16[256,256]{1,0:T(8,128)(2,1)S(1)} %get-tuple-element.10.refs_2_, ...), custom_call_target="tpu_custom_call" | custom-call | flops 1000000 | bytes 4000000 | tf_op jit(solution)/shard_map/pallas_call | solution.py:883

commit v6 on v5

--- a/solution.py
+++ b/solution.py
@@ -335,47 +335,55 @@
     carried = jnp.where(home, c, 2)
     reach = 3
 
-    def down(b, part):
-        return remote(dn_out.at[b, part], up_in.at[b, part], dn_send, up_recv.at[b, part], me - 2)
-
-    def gk_hop(b, sems, target):
-        return remote(gkb.at[b, carried], gkb.at[b, carried], sems, gk_recv.at[b, 1], target)
-
-    def gk_give(b, sems, target, to):
-        return remote(gkb.at[b, carried], gkb.at[b, c], sems, gk_recv.at[b, 0], target, to)
-
-    def gk_deliver(b, act):
-        act(gk_give(b, gk_cross, mate, 2 * x + y))
+    def sub_rows(sub):
+        return pl.ds(sub * (hrows // 2), hrows // 2)
+
+    def down(b, part, sub):
+        rows_at = sub_rows(sub) if part == 0 else pl.ds(0, hrows)
+        at = sub if part == 0 else 2
+        return remote(
+            dn_out.at[b, part, rows_at], up_in.at[b, part, rows_at], dn_send, up_recv.at[b, at], me - 2
+        )
+
+    def gk_hop(b, sub, sems, target):
+        piece = gkb.at[b, carried, sub_rows(sub)]
+        return remote(piece, piece, sems, gk_recv.at[b, 1 + sub], target)
+
+    def gk_give(b, sub, sems, target, to):
+        return remote(
+            gkb.at[b, carried, sub_rows(sub)], gkb.at[b, c, sub_rows(sub)], sems, gk_recv.at[b, 0], target, to
+        )
+
+    def gk_deliver(b, sub):
+        gk_give(b, sub, gk_cross, mate, 2 * x + y).start()
 
         @pl.when(~home)
         def _():
-            act(gk_give(b, gk_pair, me, pair))
-
-    def gk_up_near(b):
+            gk_give(b, sub, gk_pair, me, pair).start()
+
+    def gk_up_near(b, sub):
         dist = (o - b // 2) % reach
 
         @pl.when(has_up & ((dist == 0) | ((dist == 1) & (o + 2 < outer))))
         def _():
-            gk_hop(b, gk_up, me + 2).start()
+            gk_hop(b, sub, gk_up, me + 2).start()
 
     def gk_up_far(b):
         root = (o - b // 2) % reach == 0
 
-        @pl.when(root & (o + 3 < outer))
-        def _():
-            gk_hop(b, gk_up, me + 6).start()
-
-        @pl.when(root & (o + 3 == outer))
-        def _():
-            gk_hop(b, gk_up, me + 4).start()
-
-    def gk_dn_hop(b, act):
+        for sub in range(2):
+            @pl.when(root & (o + 3 < outer))
+            def _():
+                gk_hop(b, sub, gk_up, me + 6).start()
+
+            @pl.when(root & (o + 3 == outer))
+            def _():
+                gk_hop(b, sub, gk_up, me + 4).start()
+
+    def gk_dn_hop(b, sub):
         @pl.when(o > 0)
         def _():
-            act(gk_hop(b, gk_dn, me - 2))
-
-    def start(copy):
-        copy.start()
+            gk_hop(b, sub, gk_dn, me - 2).start()
 
     def gv_give(s):
         return remote(gv_fin.at[s], gv_in.at[c], gv_send.at[s], gv_recv.at[c], 2 * o + s, 2 * x + y)
@@ -389,41 +397,45 @@
         if part == 0:
             landed(p_in.at[b], p_recv.at[b])
 
-        @pl.when(has_up)
-        def _():
-            landed(up_in.at[b, part], up_recv.at[b, part])
-            keep[b, part] += up_in[b, part].astype(jnp.float32)
-
-        total = keep[b, part] + p_in[b, part].astype(jnp.float32)
-
-        @pl.when(b // 2 < o)
-        def _():
-            dn_out[b, part] = total.astype(jnp.bfloat16)
-            down(b, part).start()
-
-        @pl.when(b // 2 == o)
-        def _():
-            if part == 0:
-                gkb[b, carried] = (total * SCALE).astype(jnp.bfloat16)
-                gk_up_near(b)
-
-                @pl.when(b % 2 != y)
-                def _():
-                    each_of(o, gk_up_far)
-
-                gk_dn_hop(b, start)
-                gk_deliver(b, start)
-            else:
-                s = b % 2
-
-                @pl.when(home & (s == y))
-                def _():
-                    gv_in[c] = total.astype(jnp.bfloat16)
-
-                @pl.when(~(home & (s == y)))
-                def _():
-                    gv_fin[s] = total.astype(jnp.bfloat16)
-                    gv_give(s).start()
+        for sub in range(2 if part == 0 else 1):
+            rows_at = sub_rows(sub) if part == 0 else pl.ds(0, hrows)
+
+            @pl.when(has_up)
+            def _():
+                landed(up_in.at[b, part, rows_at], up_recv.at[b, sub if part == 0 else 2])
+                keep[b, part, rows_at] += up_in[b, part, rows_at].astype(jnp.float32)
+
+            total = keep[b, part, rows_at] + p_in[b, part, rows_at].astype(jnp.float32)
+
+            @pl.when(b // 2 < o)
+            def _():
+                dn_out[b, part, rows_at] = total.astype(jnp.bfloat16)
+                down(b, part, sub).start()
+
+            @pl.when(b // 2 == o)
+            def _():
+                if part == 0:
+                    gkb[b, carried, rows_at] = (total * SCALE).astype(jnp.bfloat16)
+                    gk_up_near(b, sub)
+
+                    if sub == 1:
+                        @pl.when(b % 2 != y)
+                        def _():
+                            each_of(o, gk_up_far)
+
+                    gk_dn_hop(b, sub)
+                    gk_deliver(b, sub)
+                else:
+                    s = b % 2
+
+                    @pl.when(home & (s == y))
+                    def _():
+                        gv_in[c] = total.astype(jnp.bfloat16)
+
+                    @pl.when(~(home & (s == y)))
+                    def _():
+                        gv_fin[s] = total.astype(jnp.bfloat16)
+                        gv_give(s).start()
 
     def sums(level, part):
         each_of(level, lambda b: reduce(b, part))
@@ -480,11 +492,38 @@
     def _():
         hid_down(0, o + 1, 1 - y)
 
+    def gq_give(s):
+        return remote(gq_fin.at[s], gq_in.at[c], gq_send.at[s], gq_recv.at[c], 2 * o + s, 2 * x + y)
+
+    def gq_part(k):
+        s = jnp.where(k == 0, 1 - y, y)
+        local = home & (s == y)
+        for at in range(2 * half):
+            cols = slice(at * HEAD_DIM, (at + 1) * HEAD_DIM)
+            piece = (gq_t[s, cols, :] * SCALE).T.astype(jnp.bfloat16)
+
+            @pl.when(local)
+            def _():
+                gq_in[c, :, cols] = piece
+
+            @pl.when(~local)
+            def _():
+                gq_fin[s, :, cols] = piece
+
+        @pl.when(~local)
+        def _():
+            gq_give(s).start()
+
     def own_level():
         kv_wait(mate, 1 - c)
         hold(1 - y, grads(mate, [1 - y], True), False)
         top_reduce(count - 1)
         hold(0, grads(2 * o, [1]), True)
+
+        @pl.when(~has_up)
+        def _():
+            gq_part(0)
+
         emit(2 * o, held(0))
         emit(2 * o + 1, held(1))
 
@@ -556,28 +595,9 @@
         def _():
             sums(0, 1)
 
-    def gq_give(s):
-        return remote(gq_fin.at[s], gq_in.at[c], gq_send.at[s], gq_recv.at[c], 2 * o + s, 2 * x + y)
-
-    @pl.loop(0, 2)
+    @pl.loop(jnp.where(has_up, 0, 1), 2)
     def _(k):
-        s = jnp.where(k == 0, 1 - y, y)
-        local = home & (s == y)
-        for at in range(2 * half):
-            cols = slice(at * HEAD_DIM, (at + 1) * HEAD_DIM)
-            piece = (gq_t[s, cols, :] * SCALE).T.astype(jnp.bfloat16)
-
-            @pl.when(local)
-            def _():
-                gq_in[c, :, cols] = piece
-
-            @pl.when(~local)
-            def _():
-                gq_fin[s, :, cols] = piece
-
-        @pl.when(~local)
-        def _():
-            gq_give(s).start()
+        gq_part(k)
 
     def hid_relay():
         hid_to_pair(0).start()
@@ -598,18 +618,22 @@
         hid_below(o)
 
     def gk_step(b):
-        landed(gkb.at[b, carried], gk_recv.at[b, 1])
+        for sub in range(2):
+            landed(gkb.at[b, carried, sub_rows(sub)], gk_recv.at[b, 1 + sub])
+
+            @pl.when(b // 2 < o)
+            def _():
+                gk_up_near(b, sub)
+
+            @pl.when(b // 2 > o)
+            def _():
+                gk_dn_hop(b, sub)
+
+            gk_deliver(b, sub)
 
         @pl.when(b // 2 < o)
         def _():
-            gk_up_near(b)
             gk_up_far(b)
-
-        @pl.when(b // 2 > o)
-        def _():
-            gk_dn_hop(b, start)
-
-        gk_deliver(b, start)
 
     def gk_ready(b):
         @pl.when(home)
@@ -855,8 +879,8 @@
         *[DMA] * 3,
         DMA((n,)),
         DMA,
-        DMA((n, 2)),
-        DMA((n, 2)),
+        DMA((n, 3)),
+        DMA((n, 3)),
         *[DMA] * 4,
         *[DMA((2,))] * 4,
         DMA,

time: 55.8 us -> 55.5 us (level)
  no operation moved by 1% of the time
where the time goes in v6:
time: 55.5 us; the launch traced here: 55.3 us
  Pallas kernels  54.6 us (98%)
  between operations  0.64 us (1%)
    pallas_call x1, Pallas kernels, on_device(): pl.pallas_call(functools.partial(attend_kernel, n, tp_count, heads), out_...  53.5 us

profile of v6, /device:TPU:25, one launch (start us, length us, event | category | flops | bytes accessed | tf_op | source)
XLA Modules:
  0.0 55.3 jit_solution(8408051806438083376)
XLA Ops:
  0.6 53.5 %shard_map.120 = (bf16[256,1024]{1,0:T(8,128)(2,1)S(1)}, bf16[256,256]{1,0:T(8,128)(2,1)S(1)}, bf16[256,256]{1,0:T(8,128)(2,1)S(1)}, f32[512,256]{1,0:T(8,128)S(1)}) custom-call(bf16[256,4096]{1,0:T(8,128)(2,1)} %hidden_ref.1, bf16[4096,256]{1,0:T(8,128)(2,1)} %weight_ref.1, bf16[256,256]{1,0:T(8,128)(2,1)} %values_ref.1, bf16[256,1024]{1,0:T(8,128)(2,1)} %q_in_ref.1, ...), custom_call_target="tpu_custom_call" | custom-call | flops 5000000000 | bytes 10000000 | tf_op jit(solution)/shard_map/pallas_call | solution.py:891
  54.2 1.1 %shard_map.121 = (bf16[256,1024]{1,0:T(8,128)(2,1)}, bf16[256,256]{1,0:T(8,128)(2,1)}, bf16[256,256]{1,0:T(8,128)(2,1)}, f32[512,256]{1,0:T(8,128)}) custom-call(bf16[256,1024]{1,0:T(8,128)(2,1)S(1)} %get-tuple-element.8.refs_0_, bf16[256,256]{1,0:T(8,128)(2,1)S(1)} %get-tuple-element.9.refs_1_, bf16[256,256]{1,0:T(8,128)(2,1)S(1)} %get-tuple-element.10.refs_2_, ...), custom_call_target="tpu_custom_call" | custom-call | flops 1000000 | bytes 4000000 | tf_op jit(solution)/shard_map/pallas_call | solution.py:907
